TPU v7x, 32 devices: a whole 2x2x4 slice. The times are simulated.
32 devices in a mesh: grp: 2 (over y), sp: 4 (over z), tp: 4 (over x, core).
Axes of the slice: x: 2, y: 2, z: 4, core: 2. Of those that a mesh axis runs over, the one named last changes fastest.
Arguments:
- inputs: bfloat16 [2048, 2048], P(('grp', 'sp')), parts along dimension 0, may hold values from -6 to 6
- norm_gain: float32 [2048], replicated, may hold values from 0.1 to 1.9
- da_query_weight: bfloat16 [2048, 1024], P('sp', 'tp'), may hold values from -0.125 to 0.125
- da_key_weight: bfloat16 [2048, 1024], P('sp', 'tp'), may hold values from -0.125 to 0.125
- da_value_weight: bfloat16 [2048, 1024], P('sp', 'tp'), may hold values from -0.125 to 0.125
- sw_query_weight: bfloat16 [2048, 1024], P('sp', 'tp'), may hold values from -0.125 to 0.125
- sw_key_weight: bfloat16 [2048, 512], P('sp', 'tp'), may hold values from -0.125 to 0.125
- sw_value_weight: bfloat16 [2048, 512], P('sp', 'tp'), may hold values from -0.125 to 0.125
- da_query_gain: float32 [64], replicated, may hold values from 0.6 to 30
- da_key_gain: float32 [64], replicated, may hold values from 0.6 to 30
- sw_query_gain: float32 [64], replicated, may hold values from 0.6 to 30
- sw_key_gain: float32 [64], replicated, may hold values from 0.6 to 30
- mix_lambda: float32 [8], P('tp'), may hold values from 0.3 to 0.8
- head_gain: float32 [128], replicated, may hold values from 0.1 to 1.9
- sink_logit: float32 [16], P('tp'), may hold values from 0 to 8
- da_out_weight: bfloat16 [1024, 2048], P('tp'), may hold values from -0.1875 to 0.1875
- sw_out_weight: bfloat16 [1024, 2048], P('tp'), may hold values from -0.1875 to 0.1875
Outputs:
- mixed: bfloat16 [2048, 2048], P(('grp', 'sp')), parts along dimension 0
There are 2 independent parts, one for each index of `grp`. A program takes and returns all parts, laid end to end along the dimension named above; an argument that names none is the same for every part. Nothing has to cross between parts.
All inputs are finite; a program needn't handle non-finite values.
Results may differ from a plain program's by a relative error of at most 0.014.
The roundings to bfloat16 on the way count: a program that leaves them out, or rounds other values in their place, can miss the bound.
Values may be sent and summed in bfloat16 or wider, within the bound.
A program may use at most 64 MiB of HBM per device.

v0:
```python
import functools

import jax
import jax.numpy as jnp
from jax import lax
from jax.experimental import pallas as pl
from jax.experimental.pallas import tpu as pltpu
from jax.sharding import PartitionSpec as P

HD = 64
WINDOW = 128


def shifted(value, axis, steps):
    count = lax.axis_size(axis)
    first, last = (max(0, -steps), min(count, count - steps))
    return lax.ppermute(value, axis, [(source, source + steps) for source in range(first, last)])


def rms_norm(values, gain):
    return values * lax.rsqrt(jnp.mean(values * values, axis=-1, keepdims=True) + 1e-06) * gain


def absorb(state, queries, places, keys, values, key_places):
    top, total, summed = state
    scores = jnp.einsum(
        "qhmd,khmd->hmqk", queries, keys, preferred_element_type=jnp.float32
    ) * HD ** (-0.5)
    scores = jnp.where(key_places[None, :] <= places[:, None], scores, -jnp.inf)
    new_top = jnp.maximum(top, jnp.max(scores, axis=-1))
    weights = jnp.exp(scores - new_top[..., None])
    total = jnp.sum(weights, axis=-1)
    summed = jnp.einsum(
        "hmqk,khe->hmqe", weights.astype(jnp.bfloat16), values, preferred_element_type=jnp.float32
    )
    return (new_top, total, summed)


def keep(state, queries, places, keys, values, key_places):
    return state


def diff_attention(queries, places, da_key, da_value, mix_lambda, head_gain):
    rows = queries.shape[0]
    heads = queries.shape[1]
    half = rows // 2
    fresh = (
        jnp.full((heads, 2, half), -1e30, jnp.float32),
        jnp.zeros((heads, 2, half), jnp.float32),
        jnp.zeros((heads, 2, half, 2 * HD), jnp.float32),
    )
    states = (fresh, fresh)
    start = jnp.int32(0)
    keys = lax.all_gather(da_key, "sp", axis=0, tiled=True)
    values = lax.all_gather(da_value, "sp", axis=0, tiled=True)
    key_places = jnp.arange(keys.shape[0], dtype=jnp.int32)
    updated = []
    for section in range(2):
        own_rows = queries[section * half : (section + 1) * half]
        own_places = places[section * half : (section + 1) * half]
        updated.append(
            lax.cond(
                start <= jnp.max(own_places),
                absorb,
                keep,
                states[section],
                own_rows,
                own_places,
                keys,
                values,
                key_places,
            )
        )
    states = tuple(updated)
    blended = []
    for top, total, summed in states:
        maps = summed / total[..., None]
        blended.append(maps[:, 0] - mix_lambda[:, None, None] * maps[:, 1])
    blend = jnp.transpose(jnp.concatenate(blended, axis=1), (1, 0, 2))
    return rms_norm(blend, head_gain).astype(jnp.bfloat16).reshape(rows, heads * 2 * HD)


def window_attention(sw_query, sw_key, sw_value, earlier_key, earlier_value, sink_logit, first):
    rows = sw_query.shape[0]
    sw_heads = sw_query.shape[1]
    kv_heads = sw_key.shape[1]
    groups = sw_heads // kv_heads
    count = rows // WINDOW

    def band(own, earlier_tile):
        tiles = own.reshape(count, WINDOW, kv_heads, HD)
        earlier = jnp.concatenate([earlier_tile[None], tiles[:-1]], axis=0)
        return jnp.concatenate([earlier, tiles], axis=1)

    key_band = band(sw_key, earlier_key)
    value_band = band(sw_value, earlier_value)
    query_tiles = sw_query.reshape(count, WINDOW, kv_heads, groups, HD)
    scores = jnp.einsum(
        "nqhgd,nkhd->nhgqk", query_tiles, key_band, preferred_element_type=jnp.float32
    ) * HD ** (-0.5)
    lag = WINDOW + jnp.arange(WINDOW)[:, None] - jnp.arange(2 * WINDOW)[None, :]
    key_places = (
        first + jnp.arange(count)[:, None] * WINDOW - WINDOW + jnp.arange(2 * WINDOW)[None, :]
    )
    valid = ((lag >= 0) & (lag < WINDOW))[None] & (key_places >= 0)[:, None, :]
    scores = jnp.where(valid[:, None, None], scores, -jnp.inf)
    sink = sink_logit.reshape(kv_heads, groups)[None, :, :, None]
    top = jnp.maximum(jnp.max(scores, axis=-1), sink)
    weights = jnp.exp(scores - top[..., None])
    total = jnp.sum(weights, axis=-1) + jnp.exp(sink - top)
    summed = jnp.einsum(
        "nhgqk,nkhd->nqhgd",
        weights.astype(jnp.bfloat16),
        value_band,
        preferred_element_type=jnp.float32,
    )
    return (
        (summed / jnp.transpose(total, (0, 3, 1, 2))[..., None])
        .astype(jnp.bfloat16)
        .reshape(rows, sw_heads * HD)
    )


def on_device(
    inputs,
    norm_gain,
    da_query_weight,
    da_key_weight,
    da_value_weight,
    sw_query_weight,
    sw_key_weight,
    sw_value_weight,
    da_query_gain,
    da_key_gain,
    sw_query_gain,
    sw_key_gain,
    mix_lambda,
    head_gain,
    sink_logit,
    da_out_weight,
    sw_out_weight,
):
    rows = inputs.shape[0]
    normed = rms_norm(inputs.astype(jnp.float32), norm_gain).astype(jnp.bfloat16)
    pieces = (
        lax.all_gather(da_query_weight, "sp", axis=0, tiled=True),
        lax.all_gather(da_key_weight, "sp", axis=0, tiled=True),
        lax.all_gather(da_value_weight, "sp", axis=0, tiled=True),
        lax.all_gather(sw_query_weight, "sp", axis=0, tiled=True),
        lax.all_gather(sw_key_weight, "sp", axis=0, tiled=True),
        lax.all_gather(sw_value_weight, "sp", axis=0, tiled=True),
    )
    projected = tuple(
        (jnp.dot(normed, piece, preferred_element_type=jnp.float32) for piece in pieces)
    )
    da_heads = da_query_weight.shape[1] // (2 * HD)
    sw_heads = sw_query_weight.shape[1] // HD
    kv_heads = sw_key_weight.shape[1] // HD
    da_query = rms_norm(projected[0].reshape(rows, da_heads, 2, HD), da_query_gain).astype(
        jnp.bfloat16
    )
    da_key = rms_norm(projected[1].reshape(rows, da_heads, 2, HD), da_key_gain).astype(jnp.bfloat16)
    da_value = projected[2].astype(jnp.bfloat16).reshape(rows, da_heads, 2 * HD)
    sw_query = rms_norm(projected[3].reshape(rows, sw_heads, HD), sw_query_gain).astype(
        jnp.bfloat16
    )
    sw_key = rms_norm(projected[4].reshape(rows, kv_heads, HD), sw_key_gain).astype(jnp.bfloat16)
    sw_value = projected[5].astype(jnp.bfloat16).reshape(rows, kv_heads, HD)
    place = lax.axis_index("sp")
    first = place * rows
    earlier_key, earlier_value = shifted(
        (sw_key[rows - WINDOW :], sw_value[rows - WINDOW :]), "sp", 1
    )
    sw_rows = window_attention(
        sw_query, sw_key, sw_value, earlier_key, earlier_value, sink_logit, first
    )
    places = first + jnp.arange(rows, dtype=jnp.int32)
    da_rows = diff_attention(da_query, places, da_key, da_value, mix_lambda, head_gain)
    partial_value = jnp.dot(da_rows, da_out_weight, preferred_element_type=jnp.float32) + jnp.dot(
        sw_rows, sw_out_weight, preferred_element_type=jnp.float32
    )
    return lax.psum(partial_value.astype(jnp.bfloat16), "tp")


MESH = pl.DeviceIdType.MESH
F32, BF16 = jnp.float32, jnp.bfloat16
CORES = 2


def dot(a, b):
    return jnp.dot(a, b, preferred_element_type=F32)


def dot_t(a, b):
    return lax.dot_general(a, b, (((1,), (1,)), ((), ())), preferred_element_type=F32)


def pair_norm(values, gain):
    lane = lax.broadcasted_iota(jnp.int32, values.shape, 1)
    squares = values * values
    low = jnp.sum(jnp.where(lane < HD, squares, 0.0), axis=-1, keepdims=True)
    high = jnp.sum(jnp.where(lane < HD, 0.0, squares), axis=-1, keepdims=True)
    mean = jnp.where(lane < HD, low, high) * (1.0 / HD)
    return values * lax.rsqrt(mean + 1e-06) * gain


def kernel(
    n,
    x_ref,
    da_q_ref,
    da_k_ref,
    da_v_ref,
    sw_q_ref,
    sw_k_ref,
    sw_v_ref,
    norm_gain_ref,
    da_q_gain_ref,
    da_k_gain_ref,
    sw_q_gain_ref,
    sw_k_gain_ref,
    head_gain_ref,
    mix_ref,
    sink_ref,
    da_out_hbm,
    sw_out_hbm,
    out_ref,
    da_out_ref,
    sw_out_ref,
    wp,
    gains_ref,
    xg,
    wb,
    normed,
    query,
    kv,
    scal,
    rows_out,
    rows_in,
    part_out,
    part_in,
    sum_out,
    sum_in,
    local_sem,
    x_send,
    x_recv,
    xf_send,
    xf_recv,
    w_send,
    w_recv,
    wy_send,
    wy_recv,
    wc_send,
    wc_recv,
    own_send,
    own_recv,
    kv_send,
    kv_recv,
    sc_send,
    sc_recv,
    r_send,
    r_recv,
    p_send,
    p_recv,
    s_send,
    s_recv,
    o_send,
    o_recv,
):
    y = lax.axis_index("grp")
    z = lax.axis_index("sp")
    t = lax.axis_index("tp")
    x = t // CORES
    c = t % CORES
    peer = {"tp": x * CORES + 1 - c}
    across = {"tp": (1 - x) * CORES + c}
    beside = {"grp": 1 - y}

    def at(zz, cc):
        return {"sp": zz, "tp": x * CORES + cc}

    def remote(src, dst, send, recv, device):
        return pltpu.make_async_remote_copy(
            src_ref=src,
            dst_ref=dst,
            send_sem=send,
            recv_sem=recv,
            device_id=device,
            device_id_type=MESH,
        )

    barrier = pltpu.get_barrier_semaphore()

    def greet(device):
        pl.semaphore_signal(barrier, inc=1, device_id=device, device_id_type=MESH)

    greet(peer)
    greet(across)
    greet(beside)
    for k in range(1, n):
        for cc in range(CORES):
            greet(at(lax.rem(z + k, n), cc))

    own_x = pltpu.make_async_copy(x_ref.at[c], xg.at[z], local_sem.at[1])
    own_x.start()
    out_loads = [
        pltpu.make_async_copy(da_out_hbm, da_out_ref, local_sem.at[4]),
        pltpu.make_async_copy(sw_out_hbm, sw_out_ref, local_sem.at[5]),
    ]
    for load in out_loads:
        load.start()

    wide = 2 * HD
    packs = []
    for par in range(CORES):
        for j, ref in enumerate((da_q_ref, da_k_ref, da_v_ref, sw_q_ref)):
            packs.append(
                pltpu.make_async_copy(
                    ref.at[:, :, :, :, pl.ds(par * wide, wide)],
                    wp.at[par, :, :, :, :, pl.ds(j * wide, wide)],
                    local_sem.at[6 + par * 4 + j],
                )
            )
    for pack in packs:
        pack.start()

    for par in range(CORES):
        cols = slice(par * HD, (par + 1) * HD)
        wp[par, :, :, :, :, 4 * wide : 5 * wide] = jnp.concatenate([sw_k_ref[..., cols], sw_v_ref[..., cols]], axis=-1)
        scal[c, par, 0:1, :] = jnp.broadcast_to(mix_ref[:, par : par + 1], (1, wide))
        for g in range(2):
            sink = sink_ref[:, 2 * par + g : 2 * par + g + 1]
            scal[c, par, 1 + g : 2 + g, :] = jnp.broadcast_to(sink, (1, wide))
    for i, ref in enumerate((da_q_gain_ref, da_k_gain_ref, sw_q_gain_ref, sw_k_gain_ref)):
        gains_ref[i : i + 1, :] = jnp.concatenate([ref[...], ref[...]], axis=-1)
    gains_ref[4:5, :] = head_gain_ref[...]
    pl.semaphore_wait(barrier, 3 + (n - 1) * CORES)

    pending = []

    def go(copy, when=None):
        if when is None:
            copy.start()
        else:
            pl.when(when)(copy.start)
        pending.append((copy, when))

    pieces = xg.shape[2]

    def hop(d, k, p):
        source = z - k if d == 0 else z + k
        source = jnp.clip(source, 0, n - 1)
        target = jnp.clip(z + 1 if d == 0 else z - 1, 0, n - 1)
        src = xg.at[source, x, p]
        return remote(
            src, xg.at[source, x, p], x_send.at[d, k, p], x_recv.at[d, k, p], {"sp": target}
        )

    def can_hop(d, k):
        return (z - k >= 0) & (z + 1 < n) if d == 0 else (z + k < n) & (z >= 1)

    def has(d, k):
        return z - k >= 0 if d == 0 else z + k < n

    def from_there(d, k):
        return jnp.clip(z - k if d == 0 else z + k, 0, n - 1)

    own_x.wait()
    for p in range(pieces):
        for d in range(2):
            go(hop(d, 0, p), can_hop(d, 0))

    owner = c == z // CORES

    for pack in packs:
        pack.wait()
    own = remote(wp.at[z % CORES], wb.at[z], own_send, own_recv, peer)
    own_local = pltpu.make_async_copy(wp.at[z % CORES], wb.at[z], local_sem.at[0])

    sc = remote(scal.at[c], scal.at[c], sc_send, sc_recv, peer)
    go(sc)

    def cross(zs, p):
        return remote(
            xg.at[zs, x, p], xg.at[zs, x, p], xf_send.at[zs, p], xf_recv.at[zs, p], across
        )

    def weight_direct(zs, s):
        return remote(
            wb.at[zs, y, c, s], wb.at[zs, y, c, s], w_send.at[0, 0, s], w_recv.at[zs, s], peer
        )

    def weight_beside(zs, yy, s):
        return remote(
            wb.at[zs, yy, c, s], wb.at[zs, yy, c, s], wy_send.at[zs, s], wy_recv.at[zs, s], beside
        )

    def weight_core(zs, which, cc, s):
        ref = wb.at[zs, y if which == 0 else 1 - y, cc, s]
        return remote(ref, ref, wc_send.at[which, zs, s], wc_recv.at[which, zs, s], peer)

    def pass_on(k, p):
        for d in range(2):
            zs = from_there(d, k)

            def arrived(zs=zs, d=d):
                remote(
                    xg.at[zs, x, p],
                    xg.at[zs, x, p],
                    x_send.at[d, k - 1, p],
                    x_recv.at[d, k - 1, p],
                    across,
                ).wait_recv()

            pl.when(has(d, k))(arrived)
            if k < n - 1:
                go(hop(d, k, p), can_hop(d, k))
            go(cross(zs, p), has(d, k))

    def send_weights(s):
        for par in range(CORES):
            zt = CORES * c + par
            for cd in range(CORES):
                go(
                    remote(
                        wp.at[par, y, cd, s],
                        wb.at[z, y, cd, s],
                        w_send.at[par, cd, s],
                        w_recv.at[z, s],
                        at(zt, cd),
                    ),
                    zt != z,
                )

    def pass_weights(k, s):
        for d in range(2):
            zs = from_there(d, k)
            pl.when(has(d, k))(lambda zs=zs: weight_direct(zs, s).wait_recv())
            go(weight_beside(zs, y, s), has(d, k))
            go(weight_core(zs, 0, c, s), has(d, k))

    def pass_beside(k, s):
        for d in range(2):
            zs = from_there(d, k)
            pl.when(has(d, k))(lambda zs=zs: weight_beside(zs, 1 - y, s).wait_recv())
            go(weight_core(zs, 1, c, s), has(d, k))

    part = xg.shape[2] * xg.shape[3]
    tile = 2 * part

    def norm_of(i):
        for h in range(2):
            values = xg[i, h].reshape(part, xg.shape[4]).astype(F32)
            values = rms_norm(values, norm_gain_ref[...])
            normed[i, h * part : (h + 1) * part, :] = values.astype(BF16)

    others = [lax.rem(z + k, n) for k in range(1, n)]
    pl.when(owner)(own_local.start)
    go(own, owner)
    for p in range(pieces):
        send_weights(p)
    for p in range(pieces):
        pass_on(1, p)
    for p in range(pieces):
        for k in range(1, n):
            pass_weights(k, p)
        if p:
            pass_on(2, p - 1)
    pass_on(2, pieces - 1)
    norm_of(z)
    for p in range(pieces):
        pass_on(3, p)
    for p in range(pieces):
        for k in range(1, n):
            pass_beside(k, p)

    for k in range(1, n):
        for d in range(2):

            @pl.when(has(d, k))
            def _(zs=from_there(d, k)):
                for p in range(pieces):
                    remote(
                        xg.at[zs, 1 - x, p],
                        xg.at[zs, 1 - x, p],
                        xf_send.at[zs, p],
                        xf_recv.at[zs, p],
                        across,
                    ).wait_recv()
                norm_of(zs)

    pl.when(owner)(own_local.wait)
    pl.when(jnp.logical_not(owner))(own.wait_recv)
    for zs in others:
        for which in range(2):
            for p in range(pieces):
                weight_core(zs, which, 1 - c, p).wait_recv()

    depth = wb.shape[1] * wb.shape[2] * wb.shape[3] * wb.shape[4]
    width = wb.shape[5]
    for i in range(n):
        acc = dot(normed[i, :, 0:depth], wb[0].reshape(depth, width))
        for j in range(1, n):
            acc += dot(normed[i, :, j * depth : (j + 1) * depth], wb[j].reshape(depth, width))
        da_q = pair_norm(acc[:, 0:wide], gains_ref[0:1, :]).astype(BF16)
        da_k = pair_norm(acc[:, wide : 2 * wide], gains_ref[1:2, :]).astype(BF16)
        da_v = acc[:, 2 * wide : 3 * wide].astype(BF16)
        sw_q = pair_norm(acc[:, 3 * wide : 4 * wide], gains_ref[2:3, :]).astype(BF16)
        sw_kv = acc[:, 4 * wide : 5 * wide]
        lane = lax.broadcasted_iota(jnp.int32, sw_kv.shape, 1)
        sw_kv = jnp.where(lane < HD, pair_norm(sw_kv, gains_ref[3:4, :]), sw_kv).astype(BF16)
        scale = jnp.asarray(HD ** (-0.5), BF16)
        query[i, :, 0:wide] = da_q * scale
        query[i, :, wide : 2 * wide] = sw_q * scale
        kv[c, i, :, 0:wide] = da_k
        kv[c, i, :, wide : 2 * wide] = da_v
        kv[c, i, :, 2 * wide : 3 * wide] = sw_kv

    swap = remote(kv.at[c], kv.at[c], kv_send, kv_recv, peer)
    go(swap)
    remote(scal.at[1 - c], scal.at[1 - c], sc_send, sc_recv, peer).wait_recv()
    remote(kv.at[1 - c], kv.at[1 - c], kv_send, kv_recv, peer).wait_recv()

    mine = scal[z // CORES, z % CORES]
    mix = mine[0:1, :]
    def send_rows(i, j):
        cols = pl.ds(j * wide, wide)
        away = (z != i) | jnp.logical_not(owner)
        go(
            remote(
                rows_out.at[i, :, cols],
                rows_in.at[z % CORES, c, :, cols],
                r_send.at[i, j],
                r_recv.at[z % CORES, c, j],
                at(i, z // CORES),
            ),
            away,
        )

    for i in range(n):
        before = jnp.maximum(i - 1 + c, 0)
        q_row = lax.broadcasted_iota(jnp.int32, (tile, tile), 0)
        k_row = lax.broadcasted_iota(jnp.int32, (tile, tile), 1)
        first_ok = (2 * i + c) > 0
        near = kv[c, i, :, 2 * wide : 3 * wide]
        far = kv[1 - c, before, :, 2 * wide : 3 * wide]
        results = []
        for g in range(2):
            q = query[i, :, wide + g * HD : wide + (g + 1) * HD]
            s_near = jnp.where(k_row <= q_row, dot_t(q, near[:, 0:HD]), -jnp.inf)
            s_far = jnp.where((k_row > q_row) & first_ok, dot_t(q, far[:, 0:HD]), -jnp.inf)
            sink = mine[1 + g : 2 + g, 0:1]
            top = jnp.maximum(
                jnp.max(s_near, axis=-1, keepdims=True), jnp.max(s_far, axis=-1, keepdims=True)
            )
            top = jnp.maximum(top, sink)
            w_near = jnp.exp(s_near - top)
            w_far = jnp.exp(s_far - top)
            total = (
                jnp.sum(w_near, axis=-1, keepdims=True)
                + jnp.sum(w_far, axis=-1, keepdims=True)
                + jnp.exp(sink - top)
            )
            summed = dot(w_near.astype(BF16), near[:, HD:wide]) + dot(
                w_far.astype(BF16), far[:, HD:wide]
            )
            results.append(summed / total)
        rows_out[i, :, wide : 2 * wide] = jnp.concatenate(results, axis=-1).astype(BF16)

        send_rows(i, 1)

    for i in range(n):
        q_place = (2 * i + c) * tile + lax.broadcasted_iota(jnp.int32, (tile, 1), 0)
        count = (i + 1) * tile
        column = lax.broadcasted_iota(jnp.int32, (1, count), 1)
        maps = []
        for m in range(2):
            q = query[i, :, m * HD : (m + 1) * HD]
            scores = []
            for h in range(2):
                keys = kv[h, 0 : i + 1, :, m * HD : (m + 1) * HD].reshape(count, HD)
                place = (column // tile) * (2 * tile) + h * tile + column % tile
                scores.append(jnp.where(place <= q_place, dot_t(q, keys), -jnp.inf))
            top = jnp.maximum(
                jnp.max(scores[0], axis=-1, keepdims=True),
                jnp.max(scores[1], axis=-1, keepdims=True),
            )
            total = 0.0
            summed = 0.0
            for h in range(2):
                weights = jnp.exp(scores[h] - top)
                total += jnp.sum(weights, axis=-1, keepdims=True)
                values = kv[h, 0 : i + 1, :, wide : 2 * wide].reshape(count, wide)
                summed += dot(weights.astype(BF16), values)
            maps.append(summed / total)
        blend = maps[0] - mix * maps[1]
        rows_out[i, :, 0:wide] = rms_norm(blend, gains_ref[4:5, :]).astype(BF16)

        send_rows(i, 0)

    keep_rows = pltpu.make_async_copy(rows_out.at[z], rows_in.at[z % CORES, c], local_sem.at[3])
    pl.when(owner)(keep_rows.start)
    pl.when(owner)(keep_rows.wait)

    def await_rows(cc):
        for par in range(CORES):

            def wait(par=par):
                for j in range(2):
                    cols = pl.ds(j * wide, wide)
                    remote(
                        rows_in.at[par, cc, :, cols],
                        rows_in.at[par, cc, :, cols],
                        r_send.at[0, j],
                        r_recv.at[par, cc, j],
                        peer,
                    ).wait_recv()

            pl.when((CORES * c + par != z) | (cc != c))(wait)

    columns = part_out.shape[1] // 4

    def project(cc, q):
        cols = slice(q * columns, (q + 1) * columns)
        acc = 0.0
        for par in range(CORES):
            rows = rows_in[par, cc]
            acc += dot(rows[:, 0:wide], da_out_ref[par * wide : (par + 1) * wide, cols])
            acc += dot(rows[:, wide : 2 * wide], sw_out_ref[par * wide : (par + 1) * wide, cols])
        return acc.astype(BF16)

    for load in out_loads:
        load.wait()
    await_rows(1 - c)
    for q in range(4 + 1):
        if q < 4:
            part_out[:, q * columns : (q + 1) * columns] = project(1 - c, q)
            cols = pl.ds(q * columns, columns)
            go(remote(part_out.at[:, cols], part_in.at[:, cols], p_send.at[q], p_recv.at[q], peer))
        if q == 0:
            await_rows(c)
            continue
        last = q - 1
        cols = pl.ds(last * columns, columns)
        mine_part = project(c, last).astype(F32)
        remote(
            part_out.at[:, cols], part_in.at[:, cols], p_send.at[last], p_recv.at[last], peer
        ).wait_recv()
        both = mine_part + part_in[:, cols].astype(F32)
        sum_out[:, cols] = both.astype(BF16)
        go(remote(sum_out.at[:, cols], sum_in.at[:, cols], s_send.at[last], s_recv.at[last], across))
    for q in range(4):
        cols = pl.ds(q * columns, columns)
        remote(sum_out.at[:, cols], sum_in.at[:, cols], s_send.at[q], s_recv.at[q], across).wait_recv()
        total = sum_out[:, cols].astype(F32) + sum_in[:, cols].astype(F32)
        out_ref[c, :, cols] = total.astype(BF16)
        go(
            remote(
                out_ref.at[c, :, cols], out_ref.at[c, :, cols], o_send.at[q], o_recv.at[q], peer
            )
        )
    for q in range(4):
        cols = pl.ds(q * columns, columns)
        remote(
            out_ref.at[1 - c, :, cols], out_ref.at[1 - c, :, cols], o_send.at[q], o_recv.at[q], peer
        ).wait_recv()
    for copy, when in pending:
        if when is None:
            copy.wait_send()
        else:
            pl.when(when)(copy.wait_send)


def transposed(n, *arrays):
    (
        inputs,
        norm_gain,
        da_query_weight,
        da_key_weight,
        da_value_weight,
        sw_query_weight,
        sw_key_weight,
        sw_value_weight,
        da_query_gain,
        da_key_gain,
        sw_query_gain,
        sw_key_gain,
        mix_lambda,
        head_gain,
        sink_logit,
        da_out_weight,
        sw_out_weight,
    ) = arrays
    rows, d = inputs.shape
    depth = da_query_weight.shape[0]
    wide = 2 * HD
    width = 5 * wide
    piece = depth // 4

    def cut(weight):
        return weight.reshape(2, CORES, pieces, piece // pieces, weight.shape[1])

    def line(vector):
        return vector.reshape(1, -1)

    pieces = 4
    part = rows // 4
    tile = rows // 2
    DMA = pltpu.SemaphoreType.DMA
    vmem = pl.BlockSpec(memory_space=pltpu.VMEM)
    hbm = pl.BlockSpec(memory_space=pl.ANY)
    out = pl.pallas_call(
        functools.partial(kernel, n),
        out_shape=jax.ShapeDtypeStruct((2, tile, d), BF16),
        in_specs=[hbm] * 5 + [vmem] * 10 + [hbm] * 2,
        out_specs=vmem,
        scratch_shapes=[
            pltpu.VMEM(da_out_weight.shape, BF16),
            pltpu.VMEM(sw_out_weight.shape, BF16),
            pltpu.VMEM((CORES, 2, CORES, pieces, piece // pieces, width), BF16),
            pltpu.VMEM((8, wide), F32),
            pltpu.VMEM((n, 2, pieces, part // pieces, d), BF16),
            pltpu.VMEM((n, 2, CORES, pieces, piece // pieces, width), BF16),
            pltpu.VMEM((n, tile, d), BF16),
            pltpu.VMEM((n, tile, 2 * wide), BF16),
            pltpu.VMEM((2, n, tile, 3 * wide), BF16),
            pltpu.VMEM((CORES, CORES, 8, wide), F32),
            pltpu.VMEM((n, tile, 2 * wide), BF16),
            pltpu.VMEM((CORES, CORES, tile, 2 * wide), BF16),
            pltpu.VMEM((tile, d), BF16),
            pltpu.VMEM((tile, d), BF16),
            pltpu.VMEM((tile, d), BF16),
            pltpu.VMEM((tile, d), BF16),
            DMA((14,)),
            DMA((2, n, pieces)),
            DMA((2, n, pieces)),
            DMA((n, pieces)),
            DMA((n, pieces)),
            DMA((CORES, CORES, pieces)),
            DMA((n, pieces)),
            DMA((n, pieces)),
            DMA((n, pieces)),
            DMA((2, n, pieces)),
            DMA((2, n, pieces)),
            DMA,
            DMA,
            DMA,
            DMA,
            DMA,
            DMA,
            DMA((n, 2)),
            DMA((CORES, CORES, 2)),
            DMA((4,)),
            DMA((4,)),
            DMA((4,)),
            DMA((4,)),
            DMA((4,)),
            DMA((4,)),
        ],
        compiler_params=pltpu.CompilerParams(
            collective_id=0, has_side_effects=True, vmem_limit_bytes=60 * 1024 * 1024
        ),
    )(
        inputs.reshape(CORES, 2, pieces, part // pieces, d),
        cut(da_query_weight),
        cut(da_key_weight),
        cut(da_value_weight),
        cut(sw_query_weight),
        cut(sw_key_weight),
        cut(sw_value_weight),
        line(norm_gain),
        line(da_query_gain),
        line(da_key_gain),
        line(sw_query_gain),
        line(sw_key_gain),
        line(head_gain),
        line(mix_lambda),
        line(sink_logit),
        da_out_weight,
        sw_out_weight,
    )
    return out.reshape(rows, d)


def body(sizes, *arrays):
    rows = arrays[0].shape[0]
    heads = arrays[12].shape[0]
    sinks = arrays[14].shape[0]
    n = sizes["sp"]
    fits = (
        sizes["grp"] == 2
        and sizes["tp"] == 2 * CORES
        and n == 2 * CORES
        and heads == CORES
        and sinks == 2 * CORES
        and arrays[6].shape[1] == CORES * HD
        and rows == 2 * WINDOW
    )
    if fits:
        return transposed(n, *arrays)
    return on_device(*arrays)


def solution(mesh):
    return jax.shard_map(
        functools.partial(body, dict(mesh.shape)),
        mesh=mesh,
        in_specs=(
            P(("grp", "sp"), None),
            P(),
            P("sp", "tp"),
            P("sp", "tp"),
            P("sp", "tp"),
            P("sp", "tp"),
            P("sp", "tp"),
            P("sp", "tp"),
            P(),
            P(),
            P(),
            P(),
            P("tp"),
            P(),
            P("tp"),
            P("tp", None),
            P("tp", None),
        ),
        out_specs=P(("grp", "sp"), None),
        check_vma=False,
    )
```

profile of v0, /device:TPU:0, one launch (start us, length us, event | category | flops | bytes accessed | tf_op | source)
XLA Modules:
  0.0 73.4 jit_solution(153374214071327091)
XLA Ops:
  0.0 71.1 %shard_map.163 = bf16[2,128,2048]{2,1,0:T(8,128)(2,1)} custom-call(bf16[2,2,4,16,2048]{4,3,2,1,0:T(8,128)(2,1)} %bitcast.17, bf16[2,2,4,32,256]{4,3,2,1,0:T(8,128)(2,1)} %bitcast.18, bf16[2,2,4,32,256]{4,3,2,1,0:T(8,128)(2,1)} %bitcast.19, bf16[2,2,4,32,256]{4,3,2,1,0:T(8,128)(2,1)} %bitcast.20, bf16[2,2,4,32,256]{4,3,2,1,0:T(8,128)(2,1)} %bitcast.21, ...), custom_call_target="tpu_custom_call" | custom-call | tf_op jit(solution)/shard_map/pallas_call | solution.py:711
  71.1 2.3 %copy.19 = bf16[256,2048]{1,0:T(8,128)(2,1)} copy(bf16[256,2048]{1,0:T(8,128)(2,1)} %bitcast.16) | data formatting | bytes 2097152
where the time goes:
time: 73.7 us; the launch traced here: 73.4 us
  Pallas kernels  71.1 us (96%)
  local copies, waits for them, and re-layouts  2.3 us (3%)
    pallas_call x1, Pallas kernels, transposed(): pl.pallas_call(functools.partial(kernel, n), out_shape=jax.ShapeDtypeStru...  71.1 us
    unnamed x1, local copies, waits for them, and re-layouts  2.3 us

commit v1 on v0

v1 whole, which is shorter than its diff:
```python
import functools

import jax
import jax.numpy as jnp
from jax import lax
from jax.experimental import pallas as pl
from jax.experimental.pallas import tpu as pltpu
from jax.sharding import PartitionSpec as P

HD = 64
WINDOW = 128


def shifted(value, axis, steps):
    count = lax.axis_size(axis)
    first, last = (max(0, -steps), min(count, count - steps))
    return lax.ppermute(value, axis, [(source, source + steps) for source in range(first, last)])


def rms_norm(values, gain):
    return values * lax.rsqrt(jnp.mean(values * values, axis=-1, keepdims=True) + 1e-06) * gain


def absorb(state, queries, places, keys, values, key_places):
    top, total, summed = state
    scores = jnp.einsum(
        "qhmd,khmd->hmqk", queries, keys, preferred_element_type=jnp.float32
    ) * HD ** (-0.5)
    scores = jnp.where(key_places[None, :] <= places[:, None], scores, -jnp.inf)
    new_top = jnp.maximum(top, jnp.max(scores, axis=-1))
    weights = jnp.exp(scores - new_top[..., None])
    total = jnp.sum(weights, axis=-1)
    summed = jnp.einsum(
        "hmqk,khe->hmqe", weights.astype(jnp.bfloat16), values, preferred_element_type=jnp.float32
    )
    return (new_top, total, summed)


def keep(state, queries, places, keys, values, key_places):
    return state


def diff_attention(queries, places, da_key, da_value, mix_lambda, head_gain):
    rows = queries.shape[0]
    heads = queries.shape[1]
    half = rows // 2
    fresh = (
        jnp.full((heads, 2, half), -1e30, jnp.float32),
        jnp.zeros((heads, 2, half), jnp.float32),
        jnp.zeros((heads, 2, half, 2 * HD), jnp.float32),
    )
    states = (fresh, fresh)
    start = jnp.int32(0)
    keys = lax.all_gather(da_key, "sp", axis=0, tiled=True)
    values = lax.all_gather(da_value, "sp", axis=0, tiled=True)
    key_places = jnp.arange(keys.shape[0], dtype=jnp.int32)
    updated = []
    for section in range(2):
        own_rows = queries[section * half : (section + 1) * half]
        own_places = places[section * half : (section + 1) * half]
        updated.append(
            lax.cond(
                start <= jnp.max(own_places),
                absorb,
                keep,
                states[section],
                own_rows,
                own_places,
                keys,
                values,
                key_places,
            )
        )
    states = tuple(updated)
    blended = []
    for top, total, summed in states:
        maps = summed / total[..., None]
        blended.append(maps[:, 0] - mix_lambda[:, None, None] * maps[:, 1])
    blend = jnp.transpose(jnp.concatenate(blended, axis=1), (1, 0, 2))
    return rms_norm(blend, head_gain).astype(jnp.bfloat16).reshape(rows, heads * 2 * HD)


def window_attention(sw_query, sw_key, sw_value, earlier_key, earlier_value, sink_logit, first):
    rows = sw_query.shape[0]
    sw_heads = sw_query.shape[1]
    kv_heads = sw_key.shape[1]
    groups = sw_heads // kv_heads
    count = rows // WINDOW

    def band(own, earlier_tile):
        tiles = own.reshape(count, WINDOW, kv_heads, HD)
        earlier = jnp.concatenate([earlier_tile[None], tiles[:-1]], axis=0)
        return jnp.concatenate([earlier, tiles], axis=1)

    key_band = band(sw_key, earlier_key)
    value_band = band(sw_value, earlier_value)
    query_tiles = sw_query.reshape(count, WINDOW, kv_heads, groups, HD)
    scores = jnp.einsum(
        "nqhgd,nkhd->nhgqk", query_tiles, key_band, preferred_element_type=jnp.float32
    ) * HD ** (-0.5)
    lag = WINDOW + jnp.arange(WINDOW)[:, None] - jnp.arange(2 * WINDOW)[None, :]
    key_places = (
        first + jnp.arange(count)[:, None] * WINDOW - WINDOW + jnp.arange(2 * WINDOW)[None, :]
    )
    valid = ((lag >= 0) & (lag < WINDOW))[None] & (key_places >= 0)[:, None, :]
    scores = jnp.where(valid[:, None, None], scores, -jnp.inf)
    sink = sink_logit.reshape(kv_heads, groups)[None, :, :, None]
    top = jnp.maximum(jnp.max(scores, axis=-1), sink)
    weights = jnp.exp(scores - top[..., None])
    total = jnp.sum(weights, axis=-1) + jnp.exp(sink - top)
    summed = jnp.einsum(
        "nhgqk,nkhd->nqhgd",
        weights.astype(jnp.bfloat16),
        value_band,
        preferred_element_type=jnp.float32,
    )
    return (
        (summed / jnp.transpose(total, (0, 3, 1, 2))[..., None])
        .astype(jnp.bfloat16)
        .reshape(rows, sw_heads * HD)
    )


def on_device(
    inputs,
    norm_gain,
    da_query_weight,
    da_key_weight,
    da_value_weight,
    sw_query_weight,
    sw_key_weight,
    sw_value_weight,
    da_query_gain,
    da_key_gain,
    sw_query_gain,
    sw_key_gain,
    mix_lambda,
    head_gain,
    sink_logit,
    da_out_weight,
    sw_out_weight,
):
    rows = inputs.shape[0]
    normed = rms_norm(inputs.astype(jnp.float32), norm_gain).astype(jnp.bfloat16)
    pieces = (
        lax.all_gather(da_query_weight, "sp", axis=0, tiled=True),
        lax.all_gather(da_key_weight, "sp", axis=0, tiled=True),
        lax.all_gather(da_value_weight, "sp", axis=0, tiled=True),
        lax.all_gather(sw_query_weight, "sp", axis=0, tiled=True),
        lax.all_gather(sw_key_weight, "sp", axis=0, tiled=True),
        lax.all_gather(sw_value_weight, "sp", axis=0, tiled=True),
    )
    projected = tuple(
        (jnp.dot(normed, piece, preferred_element_type=jnp.float32) for piece in pieces)
    )
    da_heads = da_query_weight.shape[1] // (2 * HD)
    sw_heads = sw_query_weight.shape[1] // HD
    kv_heads = sw_key_weight.shape[1] // HD
    da_query = rms_norm(projected[0].reshape(rows, da_heads, 2, HD), da_query_gain).astype(
        jnp.bfloat16
    )
    da_key = rms_norm(projected[1].reshape(rows, da_heads, 2, HD), da_key_gain).astype(jnp.bfloat16)
    da_value = projected[2].astype(jnp.bfloat16).reshape(rows, da_heads, 2 * HD)
    sw_query = rms_norm(projected[3].reshape(rows, sw_heads, HD), sw_query_gain).astype(
        jnp.bfloat16
    )
    sw_key = rms_norm(projected[4].reshape(rows, kv_heads, HD), sw_key_gain).astype(jnp.bfloat16)
    sw_value = projected[5].astype(jnp.bfloat16).reshape(rows, kv_heads, HD)
    place = lax.axis_index("sp")
    first = place * rows
    earlier_key, earlier_value = shifted(
        (sw_key[rows - WINDOW :], sw_value[rows - WINDOW :]), "sp", 1
    )
    sw_rows = window_attention(
        sw_query, sw_key, sw_value, earlier_key, earlier_value, sink_logit, first
    )
    places = first + jnp.arange(rows, dtype=jnp.int32)
    da_rows = diff_attention(da_query, places, da_key, da_value, mix_lambda, head_gain)
    partial_value = jnp.dot(da_rows, da_out_weight, preferred_element_type=jnp.float32) + jnp.dot(
        sw_rows, sw_out_weight, preferred_element_type=jnp.float32
    )
    return lax.psum(partial_value.astype(jnp.bfloat16), "tp")


MESH = pl.DeviceIdType.MESH
F32, BF16 = jnp.float32, jnp.bfloat16
CORES = 2


def dot(a, b):
    return jnp.dot(a, b, preferred_element_type=F32)


def dot_t(a, b):
    return lax.dot_general(a, b, (((1,), (1,)), ((), ())), preferred_element_type=F32)


def pair_norm(values, gain):
    lane = lax.broadcasted_iota(jnp.int32, values.shape, 1)
    squares = values * values
    low = jnp.sum(jnp.where(lane < HD, squares, 0.0), axis=-1, keepdims=True)
    high = jnp.sum(jnp.where(lane < HD, 0.0, squares), axis=-1, keepdims=True)
    mean = jnp.where(lane < HD, low, high) * (1.0 / HD)
    return values * lax.rsqrt(mean + 1e-06) * gain


PIECES = 4
CUTS = 4
HALVES = 2
COLUMNS = 4


def kernel(
    n,
    x_hbm,
    da_q_hbm,
    da_k_hbm,
    da_v_hbm,
    sw_q_hbm,
    sw_k_hbm,
    sw_v_hbm,
    norm_gain_hbm,
    da_q_gain_hbm,
    da_k_gain_hbm,
    sw_q_gain_hbm,
    sw_k_gain_hbm,
    head_gain_hbm,
    mix_hbm,
    sink_hbm,
    da_out_hbm,
    sw_out_hbm,
    out_ref,
    x_raw,
    skv_raw,
    norm_gain,
    da_q_gain,
    da_k_gain,
    sw_q_gain,
    sw_k_gain,
    head_gain,
    mix_ref,
    sink_ref,
    wout,
    wp,
    xg,
    wb,
    q_da,
    q_sw,
    kv,
    scal,
    rows_out,
    rows_in,
    sum_out,
    sum_in,
    local_sem,
    x_send,
    x_recv,
    xf_send,
    xf_recv,
    w_send,
    w_recv,
    wy_send,
    wy_recv,
    wc_send,
    wc_recv,
    own_send,
    own_recv,
    kv_send,
    kv_recv,
    sc_send,
    sc_recv,
    wo_send,
    wo_recv,
    r_send,
    r_recv,
    s_send,
    s_recv,
    o_send,
    o_recv,
):
    y = lax.axis_index("grp")
    z = lax.axis_index("sp")
    t = lax.axis_index("tp")
    x = t // CORES
    c = t % CORES
    peer = {"tp": x * CORES + 1 - c}
    across = {"tp": (1 - x) * CORES + c}
    beside = {"grp": 1 - y}
    wide = 2 * HD

    def at(zz, cc):
        return {"sp": zz, "tp": x * CORES + cc}

    def remote(src, dst, send, recv, device):
        return pltpu.make_async_remote_copy(
            src_ref=src,
            dst_ref=dst,
            send_sem=send,
            recv_sem=recv,
            device_id=device,
            device_id_type=MESH,
        )

    def go(copy, when=None):
        if when is None:
            copy.start()
        else:
            pl.when(when)(copy.start)

    barrier = pltpu.get_barrier_semaphore()

    def greet(device):
        pl.semaphore_signal(barrier, inc=1, device_id=device, device_id_type=MESH)

    for k in range(n - 1, 0, -1):
        for cc in range(CORES):
            greet(at(lax.rem(z + k, n), cc))
    greet(across)
    greet(beside)
    greet(peer)

    load_x = pltpu.make_async_copy(x_hbm.at[c], x_raw, local_sem.at[0])
    load_x.start()
    smalls = []
    for i, (source, target) in enumerate(
        (
            (norm_gain_hbm, norm_gain),
            (da_q_gain_hbm, da_q_gain),
            (da_k_gain_hbm, da_k_gain),
            (sw_q_gain_hbm, sw_q_gain),
            (sw_k_gain_hbm, sw_k_gain),
            (head_gain_hbm, head_gain),
            (mix_hbm, mix_ref),
            (sink_hbm, sink_ref),
        )
    ):
        smalls.append(pltpu.make_async_copy(source, target, local_sem.at[1 + i]))
        smalls[-1].start()
    for j, source in enumerate((sw_k_hbm, sw_v_hbm)):
        pltpu.make_async_copy(source, skv_raw.at[j], local_sem.at[9]).start()
    for par in range(CORES):
        for j, source in enumerate((da_q_hbm, da_k_hbm, da_v_hbm, sw_q_hbm)):
            pltpu.make_async_copy(
                source.at[:, :, :, :, pl.ds(par * wide, wide)],
                wp.at[par, :, :, :, :, pl.ds(j * wide, wide)],
                local_sem.at[10],
            ).start()
    for j, source in enumerate((da_out_hbm, sw_out_hbm)):
        pltpu.make_async_copy(source, wout.at[j, c], local_sem.at[11]).start()

    smalls[0].wait()
    load_x.wait()
    for h in range(2):
        for p in range(PIECES):
            values = rms_norm(x_raw[h, p].astype(F32), norm_gain[...])
            xg[z, h, p] = values.astype(BF16)
    pltpu.make_async_copy(skv_raw, skv_raw, local_sem.at[9]).wait()
    for par in range(CORES):
        cols = slice(par * HD, (par + 1) * HD)
        wp[par, :, :, :, :, 4 * wide : 5 * wide] = jnp.concatenate(
            [skv_raw[0, ..., cols], skv_raw[1, ..., cols]], axis=-1
        )
    for load in smalls[1:]:
        load.wait()
    for par in range(CORES):
        scal[c, par, 0:1, :] = jnp.broadcast_to(mix_ref[:, par : par + 1], (1, wide))
        for g in range(2):
            sink = sink_ref[:, 2 * par + g : 2 * par + g + 1]
            scal[c, par, 1 + g : 2 + g, :] = jnp.broadcast_to(sink, (1, wide))
    packed = wp.at[:, :, :, :, :, pl.ds(0, 4 * wide)]
    pltpu.make_async_copy(packed, packed, local_sem.at[10]).wait()
    pl.semaphore_wait(barrier, 3 + (n - 1) * CORES)

    def from_there(d, k):
        return jnp.clip(z - k if d == 0 else z + k, 0, n - 1)

    def has(d, k):
        return z - k >= 0 if d == 0 else z + k < n

    def can_hop(d, k):
        return (z - k >= 0) & (z + 1 < n) if d == 0 else (z + k < n) & (z >= 1)

    def hop(d, k, p):
        source = from_there(d, k)
        target = jnp.clip(z + 1 if d == 0 else z - 1, 0, n - 1)
        piece = xg.at[source, x, p]
        return remote(piece, piece, x_send.at[d], x_recv.at[d, k, p], {"sp": target})

    def cross(zs, p):
        piece = xg.at[zs, x, p]
        return remote(piece, piece, xf_send, xf_recv.at[zs], across)

    owner = c == z // CORES

    def send_weights(s):
        for par in range(CORES):
            zt = CORES * c + par
            for cd in range(CORES):
                piece = wp.at[par, y, cd, s]
                go(
                    remote(piece, wb.at[z, y, cd, s], w_send, w_recv.at[z, s], at(zt, cd)),
                    zt != z,
                )

    def weight_beside(zs, yy, s):
        piece = wb.at[zs, yy, c, s]
        return remote(piece, piece, wy_send, wy_recv.at[zs, s], beside)

    def weight_core(zs, yy, s):
        piece = wb.at[zs, yy, c, s]
        return remote(piece, piece, wc_send, wc_recv, peer)

    def event_x(d, k, p):
        zs = from_there(d, k)

        @pl.when(has(d, k))
        def _():
            piece = xg.at[zs, x, p]
            remote(piece, piece, x_send.at[d], x_recv.at[d, k - 1, p], across).wait_recv()

        if k < n - 1:
            go(hop(d, k, p), can_hop(d, k))
        go(cross(zs, p), has(d, k))

    def event_w(d, k, s):
        zs = from_there(d, k)

        @pl.when(has(d, k))
        def _():
            piece = wb.at[zs, y, c, s]
            remote(piece, piece, w_send, w_recv.at[zs, s], peer).wait_recv()
            weight_beside(zs, y, s).start()
            weight_core(zs, y, s).start()

    def event_y(d, k, s):
        zs = from_there(d, k)

        @pl.when(has(d, k))
        def _():
            weight_beside(zs, 1 - y, s).wait_recv()
            weight_core(zs, 1 - y, s).start()

    def both(event, k, p):
        for d in range(2):
            event(d, k, p)

    tile = xg.shape[1] * xg.shape[2] * xg.shape[3]
    depth = wb.shape[1] * wb.shape[2] * wb.shape[3] * wb.shape[4]
    width = wb.shape[5]

    def lanes(shape):
        return lax.broadcasted_iota(jnp.int32, shape, len(shape) - 1)

    low = lanes((tile, wide)) < HD

    def twice(ref):
        return jnp.concatenate([ref[...], ref[...]], axis=-1)

    def arrive(b):
        @pl.when(b != z)
        def _():
            block = xg.at[b, 1 - x]
            remote(block, block, xf_send, xf_recv.at[b], across).wait_recv()

    def project(b):
        block = xg[b].reshape(tile, xg.shape[4])
        acc = dot(block[:, 0:depth], wb[0].reshape(depth, width))
        for j in range(1, n):
            acc += dot(block[:, j * depth : (j + 1) * depth], wb[j].reshape(depth, width))
        scale = HD ** (-0.5)

        def heads(values, gain):
            normed = pair_norm(values, gain).astype(BF16).astype(F32) * scale
            low_half = jnp.where(low, normed, 0.0).astype(BF16)
            high_half = jnp.where(low, 0.0, normed).astype(BF16)
            return low_half, high_half

        low_half, high_half = heads(acc[:, 0:wide], twice(da_q_gain))
        q_da[b, 0] = low_half
        q_da[b, 1] = high_half
        low_half, high_half = heads(acc[:, 3 * wide : 4 * wide], twice(sw_q_gain))
        q_sw[b, 0] = low_half
        q_sw[b, 1] = high_half
        key = pair_norm(acc[:, wide : 2 * wide], twice(da_k_gain))
        kv[c, b, :, 0:wide] = key.astype(BF16)
        kv[c, b, :, wide : 2 * wide] = acc[:, 2 * wide : 3 * wide].astype(BF16)
        pair = acc[:, 4 * wide : 5 * wide]
        key = pair_norm(pair, twice(sw_k_gain))
        key = jnp.where(low, key, pltpu.roll(key, HD, 1))
        value = jnp.where(low, pltpu.roll(pair, HD, 1), pair)
        kv[c, b, :, 2 * wide : 3 * wide] = key.astype(BF16)
        kv[c, b, :, 3 * wide : 4 * wide] = value.astype(BF16)

    def swap(b, core):
        block = kv.at[core, b]
        return remote(block, block, kv_send, kv_recv.at[b], peer)

    def mine():
        return scal[z // CORES, z % CORES]

    def window(i):
        before = jnp.maximum(i - 1 + c, 0)
        q = q_sw[i].reshape(2 * tile, wide)
        near = kv[c, i, :, 2 * wide : 4 * wide]
        far = kv[1 - c, before, :, 2 * wide : 4 * wide]
        row = lax.broadcasted_iota(jnp.int32, (2 * tile, tile), 0)
        head = row[:, 0:1] < tile
        row = jnp.where(row < tile, row, row - tile)
        column = lanes((2 * tile, tile))
        first_ok = (2 * i + c) > 0
        s_near = jnp.where(column <= row, dot_t(q, near[:, 0:wide]), -jnp.inf)
        s_far = jnp.where((column > row) & first_ok, dot_t(q, far[:, 0:wide]), -jnp.inf)
        own = mine()
        sink = jnp.where(head, own[1:2, 0:1], own[2:3, 0:1])
        top = jnp.maximum(jnp.max(jnp.maximum(s_near, s_far), axis=-1, keepdims=True), sink)
        w_near = jnp.exp(s_near - top)
        w_far = jnp.exp(s_far - top)
        total = jnp.sum(w_near + w_far, axis=-1, keepdims=True) + jnp.exp(sink - top)
        summed = dot(w_near.astype(BF16), near[:, wide : 2 * wide]) + dot(
            w_far.astype(BF16), far[:, wide : 2 * wide]
        )
        result = summed / total
        return jnp.where(low, result[0:tile], result[tile : 2 * tile]).astype(BF16)

    part = tile // HALVES

    def spread(i, half):
        rows = slice(half * part, (half + 1) * part)
        size = 2 * part
        q = q_da[i, :, rows, :].reshape(size, wide)
        row = lax.broadcasted_iota(jnp.int32, (size, tile), 0)
        row = jnp.where(row < part, row, row - part) + half * part
        column = lanes((size, tile))
        scores = []
        top = None
        for h in range(2):
            keys = kv[h, 0 : i + 1, :, 0:wide].reshape((i + 1) * tile, wide)
            s = dot_t(q, keys)
            tiles = [s[:, j * tile : (j + 1) * tile] for j in range(i + 1)]
            tiles[i] = jnp.where(column + (h - c) * tile <= row, tiles[i], -jnp.inf)
            scores.append(tiles)
            for one in tiles:
                top = one if top is None else jnp.maximum(top, one)
        top = jnp.max(top, axis=-1, keepdims=True)
        total = None
        summed = None
        for h in range(2):
            weights = [jnp.exp(one - top) for one in scores[h]]
            for one in weights:
                total = one if total is None else total + one
            values = kv[h, 0 : i + 1, :, wide : 2 * wide].reshape((i + 1) * tile, wide)
            flat = jnp.concatenate([one.astype(BF16) for one in weights], axis=-1)
            step = dot(flat, values)
            summed = step if summed is None else summed + step
        total = jnp.sum(total, axis=-1, keepdims=True)
        maps = summed / total
        blend = maps[0:part] - mine()[0:1, :] * maps[part:size]
        return rms_norm(blend, head_gain[...]).astype(BF16)

    def send_rows(i, j, half):
        rows = pl.ds(half * part, part)
        go(
            remote(
                rows_out.at[i, j, rows],
                rows_in.at[j, z, rows],
                r_send,
                r_recv.at[j, half],
                {"sp": i},
            ),
            z != i,
        )

        @pl.when(z == i)
        def _():
            rows = slice(half * part, (half + 1) * part)
            rows_in[j, i, rows, :] = rows_out[i, j, rows, :]

    def await_rows(j, half):
        block = rows_in.at[j, 0 : n - 1, pl.ds(half * part, part)]
        remote(block, block, r_send, r_recv.at[j, half], peer).wait_recv()

    blocks = (
        z,
        z + 1 - 2 * (z % 2),
        jnp.where(z < 2, 2, 1),
        jnp.where(z < 2, 3, 0),
    )

    own = remote(wp.at[z % CORES], wb.at[z], own_send, own_recv, peer)
    own_local = pltpu.make_async_copy(wp.at[z % CORES], wb.at[z], local_sem.at[12])
    sc = remote(scal.at[c], scal.at[c], sc_send, sc_recv, peer)
    share = remote(wout.at[:, c], wout.at[:, c], wo_send, wo_recv, peer)

    for p in range(PIECES):
        send_weights(p)
        for d in range(2):
            go(hop(d, 0, p), can_hop(d, 0))
    go(own, jnp.logical_not(owner) if False else owner)
    pl.when(owner)(own_local.start)
    go(sc)
    pltpu.make_async_copy(wout.at[:, c], wout.at[:, c], local_sem.at[11]).wait()
    go(share)

    for p in range(PIECES):
        both(event_x, 1, p)
        for k in range(1, n):
            both(event_w, k, p)
        if p:
            for k in range(1, n):
                both(event_y, k, p - 1)
            both(event_x, 2, p - 1)
    for k in range(1, n):
        both(event_y, k, PIECES - 1)
    both(event_x, 2, PIECES - 1)
    pl.when(owner)(own_local.wait)
    pl.when(jnp.logical_not(owner))(own.wait_recv)
    theirs = wb.at[0 : n - 1, :, 1 - c]
    remote(theirs, theirs, wc_send, wc_recv, peer).wait_recv()
    project(blocks[0])
    go(swap(blocks[0], c))
    both(event_x, 3, 0)
    arrive(blocks[1])
    project(blocks[1])
    go(swap(blocks[1], c))
    both(event_x, 3, 1)
    both(event_x, 3, 2)
    both(event_x, 3, 3)
    arrive(blocks[2])
    project(blocks[2])
    go(swap(blocks[2], c))
    remote(scal.at[1 - c], scal.at[1 - c], sc_send, sc_recv, peer).wait_recv()
    for b in blocks[:3]:
        swap(b, 1 - c).wait_recv()
    early = (jnp.where(z < 2, 1, 3), 2)
    late = (jnp.where(z < 2, 0, 1), jnp.where(z < 2, 3, 0))
    for i in early:
        rows_out[i, 1] = window(i)
    arrive(blocks[3])
    project(blocks[3])
    go(swap(blocks[3], c))
    swap(blocks[3], 1 - c).wait_recv()
    for i in late:
        rows_out[i, 1] = window(i)
    for half in range(HALVES):
        rows = slice(half * part, (half + 1) * part)
        for i in range(n):
            send_rows(i, 1, half)
        for i in (3, 0, 2, 1):
            rows_out[i, 0, rows, :] = spread(i, half)
        for i in (3, 0, 2, 1):
            send_rows(i, 0, half)

    share_in = wout.at[:, 1 - c]
    remote(share_in, share_in, wo_send, wo_recv, peer).wait_recv()
    columns = out_ref.shape[2] // COLUMNS

    def span(half, q):
        return pl.ds(half * part, part), pl.ds(q * columns, columns)

    def summing(half, q):
        rows, cols = span(half, q)
        return remote(
            sum_out.at[rows, cols],
            sum_in.at[rows, cols],
            s_send,
            s_recv.at[half, q],
            across,
        )

    def finish(half, q):
        rows, cols = span(half, q)
        summing(half, q).wait_recv()
        out_ref[c, rows, cols] = (sum_out[rows, cols].astype(F32) + sum_in[rows, cols].astype(F32)).astype(BF16)
        block = out_ref.at[c, rows, cols]
        go(remote(block, block, o_send, o_recv, peer))

    for half in range(HALVES):
        rows = slice(half * part, (half + 1) * part)
        await_rows(1, half)
        await_rows(0, half)
        for q in range(COLUMNS):
            cols = slice(q * columns, (q + 1) * columns)
            acc = None
            for j in range(2):
                values = jnp.concatenate([rows_in[j, zs, rows, :] for zs in range(n)], axis=-1)
                step = dot(values, wout[j, :, :, cols].reshape(2 * wout.shape[2], columns))
                acc = step if acc is None else acc + step
            sum_out[rows, cols] = acc.astype(BF16)
            go(summing(half, q))
    for half in range(HALVES):
        for q in range(COLUMNS):
            finish(half, q)
    block = out_ref.at[1 - c]
    remote(block, block, o_send, o_recv, peer).wait_recv()

    def drained(ref, sem):
        remote(ref, ref, sem, o_recv, peer).wait_send()

    for zz in range(n):

        @pl.when(z == zz)
        def _(zz=zz):
            if zz + 1 < n:
                drained(xg.at[0 : zz + 1, x], x_send.at[0])
            if zz >= 1:
                drained(xg.at[0 : n - zz, x], x_send.at[1])

    drained(xg.at[0 : n - 1, x], xf_send)
    pl.when(owner)(lambda: drained(wp.at[0, y], w_send))
    pl.when(jnp.logical_not(owner))(lambda: drained(wp.at[:, y], w_send))
    pl.when(owner)(lambda: drained(wp.at[0], own_send))
    drained(wb.at[0 : n - 1, y, c], wy_send)
    drained(wb.at[0 : n - 1, :, c], wc_send)
    drained(scal.at[c], sc_send)
    drained(wout.at[:, c], wo_send)
    drained(kv.at[c], kv_send)
    drained(rows_out.at[0 : n - 1], r_send)
    drained(sum_out, s_send)
    drained(out_ref.at[c], o_send)


def transposed(n, *arrays):
    (
        inputs,
        norm_gain,
        da_query_weight,
        da_key_weight,
        da_value_weight,
        sw_query_weight,
        sw_key_weight,
        sw_value_weight,
        da_query_gain,
        da_key_gain,
        sw_query_gain,
        sw_key_gain,
        mix_lambda,
        head_gain,
        sink_logit,
        da_out_weight,
        sw_out_weight,
    ) = arrays
    rows, d = inputs.shape
    depth = da_query_weight.shape[0]
    wide = 2 * HD
    width = 5 * wide
    cut_rows = depth // 4 // CUTS
    tile = rows // 2
    part = tile // 2 // PIECES
    group = da_out_weight.shape[0]

    def cut(weight):
        return weight.reshape(2, CORES, CUTS, cut_rows, weight.shape[1])

    def line(vector):
        return vector.reshape(1, -1)

    DMA = pltpu.SemaphoreType.DMA
    any_space = pl.BlockSpec(memory_space=pl.ANY)
    out = pl.pallas_call(
        functools.partial(kernel, n),
        out_shape=pltpu.VMEM((2, tile, d), BF16),
        in_specs=[any_space] * 17,
        out_specs=pl.BlockSpec(memory_space=pltpu.VMEM),
        scratch_shapes=[
            pltpu.VMEM((2, PIECES, part, d), BF16),
            pltpu.VMEM((2, 2, CORES, CUTS, cut_rows, wide), BF16),
            pltpu.VMEM((1, d), F32),
            pltpu.VMEM((1, HD), F32),
            pltpu.VMEM((1, HD), F32),
            pltpu.VMEM((1, HD), F32),
            pltpu.VMEM((1, HD), F32),
            pltpu.VMEM((1, wide), F32),
            pltpu.VMEM((1, mix_lambda.shape[0]), F32),
            pltpu.VMEM((1, sink_logit.shape[0]), F32),
            pltpu.VMEM((2, CORES, group, d), BF16),
            pltpu.VMEM((CORES, 2, CORES, CUTS, cut_rows, width), BF16),
            pltpu.VMEM((n, 2, PIECES, part, d), BF16),
            pltpu.VMEM((n, 2, CORES, CUTS, cut_rows, width), BF16),
            pltpu.VMEM((n, 2, tile, wide), BF16),
            pltpu.VMEM((n, 2, tile, wide), BF16),
            pltpu.VMEM((CORES, n, tile, 4 * wide), BF16),
            pltpu.VMEM((CORES, CORES, 8, wide), F32),
            pltpu.VMEM((n, 2, tile, wide), BF16),
            pltpu.VMEM((2, n, tile, wide), BF16),
            pltpu.VMEM((tile, d), BF16),
            pltpu.VMEM((tile, d), BF16),
            DMA((14,)),
            DMA((2,)),
            DMA((2, n - 1, PIECES)),
            DMA,
            DMA((n,)),
            DMA,
            DMA((n, CUTS)),
            DMA,
            DMA((n, CUTS)),
            DMA,
            DMA,
            DMA,
            DMA,
            DMA,
            DMA((n,)),
            DMA,
            DMA,
            DMA,
            DMA,
            DMA,
            DMA((2, HALVES)),
            DMA,
            DMA((HALVES, COLUMNS)),
            DMA,
            DMA,
        ],
        compiler_params=pltpu.CompilerParams(
            collective_id=0, has_side_effects=True, vmem_limit_bytes=60 * 1024 * 1024
        ),
    )(
        inputs.reshape(CORES, 2, PIECES, part, d),
        cut(da_query_weight),
        cut(da_key_weight),
        cut(da_value_weight),
        cut(sw_query_weight),
        cut(sw_key_weight),
        cut(sw_value_weight),
        line(norm_gain),
        line(da_query_gain),
        line(da_key_gain),
        line(sw_query_gain),
        line(sw_key_gain),
        line(head_gain),
        line(mix_lambda),
        line(sink_logit),
        da_out_weight,
        sw_out_weight,
    )
    return out.reshape(rows, d)


def body(sizes, *arrays):
    rows = arrays[0].shape[0]
    heads = arrays[12].shape[0]
    sinks = arrays[14].shape[0]
    n = sizes["sp"]
    fits = (
        sizes["grp"] == 2
        and sizes["tp"] == 2 * CORES
        and n == 2 * CORES
        and heads == CORES
        and sinks == 2 * CORES
        and arrays[6].shape[1] == CORES * HD
        and rows == 2 * WINDOW
    )
    if fits:
        return transposed(n, *arrays)
    return on_device(*arrays)


def solution(mesh):
    return jax.shard_map(
        functools.partial(body, dict(mesh.shape)),
        mesh=mesh,
        in_specs=(
            P(("grp", "sp"), None),
            P(),
            P("sp", "tp"),
            P("sp", "tp"),
            P("sp", "tp"),
            P("sp", "tp"),
            P("sp", "tp"),
            P("sp", "tp"),
            P(),
            P(),
            P(),
            P(),
            P("tp"),
            P(),
            P("tp"),
            P("tp", None),
            P("tp", None),
        ),
        out_specs=P(("grp", "sp"), None),
        check_vma=False,
    )
```

time: 73.7 us -> 65.6 us (0.89)
  Pallas kernels: 71.1 us -> 64.5 us
  local copies, waits for them, and re-layouts: 2.3 us -> 0.97 us
    pallas_call x1, Pallas kernels: 71.1 us -> 64.5 us  [transposed(): pl.pallas_call(functools.partial(kernel, n), out_shape=pltpu.VMEM((2, til...]
    unnamed x1, local copies, waits for them, and re-layouts: 2.3 us -> 0.97 us
where the time goes in v1:
time: 65.6 us; the launch traced here: 65.5 us
  Pallas kernels  64.5 us (98%)
  local copies, waits for them, and re-layouts  0.97 us (1%)
    pallas_call x1, Pallas kernels, transposed(): pl.pallas_call(functools.partial(kernel, n), out_shape=pltpu.VMEM((2, til...  64.5 us

profile of v1, /device:TPU:0, one launch (start us, length us, event | category | flops | bytes accessed | tf_op | source)
XLA Modules:
  0.0 65.5 jit_solution(8354254464959223290)
XLA Ops:
  0.0 64.5 %shard_map.163 = bf16[2,128,2048]{2,1,0:T(8,128)(2,1)S(1)} custom-call(bf16[2,2,4,16,2048]{4,3,2,1,0:T(8,128)(2,1)} %bitcast.17, bf16[2,2,4,32,256]{4,3,2,1,0:T(8,128)(2,1)} %bitcast.18, bf16[2,2,4,32,256]{4,3,2,1,0:T(8,128)(2,1)} %bitcast.19, bf16[2,2,4,32,256]{4,3,2,1,0:T(8,128)(2,1)} %bitcast.20, bf16[2,2,4,32,256]{4,3,2,1,0:T(8,128)(2,1)} %bitcast.21, ...), custom_call_target="tpu_custom_call" | custom-call | tf_op jit(solution)/shard_map/pallas_call | solution.py:759
  64.5 1.0 %copy.19 = bf16[256,2048]{1,0:T(8,128)(2,1)} copy(bf16[256,2048]{1,0:T(8,128)(2,1)S(1)} %bitcast.16) | data formatting | bytes 2097152

commit v2 on v1

--- a/solution.py
+++ b/solution.py
@@ -208,6 +208,7 @@
 CUTS = 4
 HALVES = 2
 COLUMNS = 4
+SHARES = 4
 
 
 def kernel(
@@ -371,20 +372,8 @@
     pltpu.make_async_copy(packed, packed, local_sem.at[10]).wait()
     pl.semaphore_wait(barrier, 3 + (n - 1) * CORES)
 
-    def from_there(d, k):
-        return jnp.clip(z - k if d == 0 else z + k, 0, n - 1)
-
-    def has(d, k):
-        return z - k >= 0 if d == 0 else z + k < n
-
-    def can_hop(d, k):
-        return (z - k >= 0) & (z + 1 < n) if d == 0 else (z + k < n) & (z >= 1)
-
-    def hop(d, k, p):
-        source = from_there(d, k)
-        target = jnp.clip(z + 1 if d == 0 else z - 1, 0, n - 1)
-        piece = xg.at[source, x, p]
-        return remote(piece, piece, x_send.at[d], x_recv.at[d, k, p], {"sp": target})
+    def way(d):
+        return 1 - 2 * d
 
     def cross(zs, p):
         piece = xg.at[zs, x, p]
@@ -392,15 +381,11 @@
 
     owner = c == z // CORES
 
-    def send_weights(s):
-        for par in range(CORES):
-            zt = CORES * c + par
-            for cd in range(CORES):
-                piece = wp.at[par, y, cd, s]
-                go(
-                    remote(piece, wb.at[z, y, cd, s], w_send, w_recv.at[z, s], at(zt, cd)),
-                    zt != z,
-                )
+    def hop(zz, d, k, p):
+        source, target = zz - k * way(d), zz + way(d)
+        if 0 <= target < n:
+            piece = xg.at[source, x, p]
+            remote(piece, piece, x_send.at[d], x_recv.at[d, k, p], {"sp": target}).start()
 
     def weight_beside(zs, yy, s):
         piece = wb.at[zs, yy, c, s]
@@ -410,39 +395,41 @@
         piece = wb.at[zs, yy, c, s]
         return remote(piece, piece, wc_send, wc_recv, peer)
 
-    def event_x(d, k, p):
-        zs = from_there(d, k)
-
-        @pl.when(has(d, k))
-        def _():
-            piece = xg.at[zs, x, p]
-            remote(piece, piece, x_send.at[d], x_recv.at[d, k - 1, p], across).wait_recv()
-
+    def event_x(zz, d, k, p):
+        zs = zz - k * way(d)
+        piece = xg.at[zs, x, p]
+        remote(piece, piece, x_send.at[d], x_recv.at[d, k - 1, p], across).wait_recv()
         if k < n - 1:
-            go(hop(d, k, p), can_hop(d, k))
-        go(cross(zs, p), has(d, k))
-
-    def event_w(d, k, s):
-        zs = from_there(d, k)
-
-        @pl.when(has(d, k))
-        def _():
-            piece = wb.at[zs, y, c, s]
-            remote(piece, piece, w_send, w_recv.at[zs, s], peer).wait_recv()
-            weight_beside(zs, y, s).start()
-            weight_core(zs, y, s).start()
-
-    def event_y(d, k, s):
-        zs = from_there(d, k)
-
-        @pl.when(has(d, k))
-        def _():
-            weight_beside(zs, 1 - y, s).wait_recv()
-            weight_core(zs, 1 - y, s).start()
-
-    def both(event, k, p):
-        for d in range(2):
-            event(d, k, p)
+            hop(zz, d, k, p)
+        cross(zs, p).start()
+
+    def event_w(zs, s):
+        piece = wb.at[zs, y, c, s]
+        remote(piece, piece, w_send, w_recv.at[zs, s], peer).wait_recv()
+        weight_beside(zs, y, s).start()
+        weight_core(zs, y, s).start()
+
+    def event_y(zs, s):
+        weight_beside(zs, 1 - y, s).wait_recv()
+        weight_core(zs, 1 - y, s).start()
+
+    def send_weight(zz, zt, s):
+        for cd in range(CORES):
+            remote(
+                wp.at[zt % CORES, y, cd, s],
+                wb.at[zz, y, cd, s],
+                w_send,
+                w_recv.at[zz, s],
+                at(zt, cd),
+            ).start()
+
+    def run(script):
+        for zz in range(n):
+            for cc in range(CORES):
+
+                @pl.when((z == zz) & (c == cc))
+                def _(zz=zz, cc=cc):
+                    script(zz, cc)
 
     tile = xg.shape[1] * xg.shape[2] * xg.shape[3]
     depth = wb.shape[1] * wb.shape[2] * wb.shape[3] * wb.shape[4]
@@ -455,6 +442,8 @@
 
     def twice(ref):
         return jnp.concatenate([ref[...], ref[...]], axis=-1)
+
+    normed = pair_norm
 
     def arrive(b):
         @pl.when(b != z)
@@ -470,26 +459,28 @@
         scale = HD ** (-0.5)
 
         def heads(values, gain):
-            normed = pair_norm(values, gain).astype(BF16).astype(F32) * scale
-            low_half = jnp.where(low, normed, 0.0).astype(BF16)
-            high_half = jnp.where(low, 0.0, normed).astype(BF16)
+            result = normed(values, gain).astype(BF16).astype(F32) * scale
+            low_half = jnp.where(low, result, 0.0).astype(BF16)
+            high_half = jnp.where(low, 0.0, result).astype(BF16)
             return low_half, high_half
 
+        key = normed(acc[:, wide : 2 * wide], twice(da_k_gain))
+        kv[c, b, :, 0:wide] = key.astype(BF16)
+        kv[c, b, :, wide : 2 * wide] = acc[:, 2 * wide : 3 * wide].astype(BF16)
+        pair = acc[:, 4 * wide : 5 * wide]
+        pair = jnp.where(low, normed(pair, twice(sw_k_gain)), pair).astype(BF16)
+        row = lax.broadcasted_iota(jnp.int32, (wide, 2 * wide), 0)
+        column = lanes((wide, 2 * wide))
+        source = column % HD + jnp.where(column < wide, 0, HD)
+        doubler = jnp.where(row == source, 1.0, 0.0).astype(BF16)
+        kv[c, b, :, 2 * wide : 4 * wide] = dot(pair, doubler).astype(BF16)
+        swap(b, c).start()
         low_half, high_half = heads(acc[:, 0:wide], twice(da_q_gain))
         q_da[b, 0] = low_half
         q_da[b, 1] = high_half
         low_half, high_half = heads(acc[:, 3 * wide : 4 * wide], twice(sw_q_gain))
         q_sw[b, 0] = low_half
         q_sw[b, 1] = high_half
-        key = pair_norm(acc[:, wide : 2 * wide], twice(da_k_gain))
-        kv[c, b, :, 0:wide] = key.astype(BF16)
-        kv[c, b, :, wide : 2 * wide] = acc[:, 2 * wide : 3 * wide].astype(BF16)
-        pair = acc[:, 4 * wide : 5 * wide]
-        key = pair_norm(pair, twice(sw_k_gain))
-        key = jnp.where(low, key, pltpu.roll(key, HD, 1))
-        value = jnp.where(low, pltpu.roll(pair, HD, 1), pair)
-        kv[c, b, :, 2 * wide : 3 * wide] = key.astype(BF16)
-        kv[c, b, :, 3 * wide : 4 * wide] = value.astype(BF16)
 
     def swap(b, core):
         block = kv.at[core, b]
@@ -498,31 +489,49 @@
     def mine():
         return scal[z // CORES, z % CORES]
 
-    def window(i):
-        before = jnp.maximum(i - 1 + c, 0)
-        q = q_sw[i].reshape(2 * tile, wide)
-        near = kv[c, i, :, 2 * wide : 4 * wide]
-        far = kv[1 - c, before, :, 2 * wide : 4 * wide]
-        row = lax.broadcasted_iota(jnp.int32, (2 * tile, tile), 0)
-        head = row[:, 0:1] < tile
-        row = jnp.where(row < tile, row, row - tile)
-        column = lanes((2 * tile, tile))
-        first_ok = (2 * i + c) > 0
-        s_near = jnp.where(column <= row, dot_t(q, near[:, 0:wide]), -jnp.inf)
-        s_far = jnp.where((column > row) & first_ok, dot_t(q, far[:, 0:wide]), -jnp.inf)
-        own = mine()
-        sink = jnp.where(head, own[1:2, 0:1], own[2:3, 0:1])
-        top = jnp.maximum(jnp.max(jnp.maximum(s_near, s_far), axis=-1, keepdims=True), sink)
-        w_near = jnp.exp(s_near - top)
-        w_far = jnp.exp(s_far - top)
-        total = jnp.sum(w_near + w_far, axis=-1, keepdims=True) + jnp.exp(sink - top)
-        summed = dot(w_near.astype(BF16), near[:, wide : 2 * wide]) + dot(
-            w_far.astype(BF16), far[:, wide : 2 * wide]
-        )
-        result = summed / total
-        return jnp.where(low, result[0:tile], result[tile : 2 * tile]).astype(BF16)
-
     part = tile // HALVES
+
+    def windows(items, start, count):
+        rows = slice(start, start + count)
+        size = 2 * count
+        row = lax.broadcasted_iota(jnp.int32, (size, tile), 0)
+        head = row[:, 0:1] < count
+        row = jnp.where(row < count, row, row - count) + start
+        column = lanes((size, tile))
+        causal = column <= row
+        own_scal = mine()
+        sink = jnp.where(head, own_scal[1:2, 0:1], own_scal[2:3, 0:1])
+        pairs = [
+            (
+                kv[c, i, :, 2 * wide : 4 * wide],
+                kv[1 - c, jnp.maximum(i - 1 + c, 0), :, 2 * wide : 4 * wide],
+            )
+            for i in items
+        ]
+        scores = []
+        for i, (near, far) in zip(items, pairs):
+            q = q_sw[i, :, rows, :].reshape(size, wide)
+            far_ok = (column > row) & (2 * i + c > 0)
+            scores.append(
+                (
+                    jnp.where(causal, dot_t(q, near[:, 0:wide]), -jnp.inf),
+                    jnp.where(far_ok, dot_t(q, far[:, 0:wide]), -jnp.inf),
+                )
+            )
+        tops = [
+            jnp.maximum(jnp.max(jnp.maximum(*two), axis=-1, keepdims=True), sink) for two in scores
+        ]
+        weights_of = [[jnp.exp(one - top) for one in two] for two, top in zip(scores, tops)]
+        totals = [
+            jnp.sum(two[0] + two[1], axis=-1, keepdims=True) + jnp.exp(sink - top)
+            for two, top in zip(weights_of, tops)
+        ]
+        low_part = lanes((count, wide)) < HD
+        for i, (near, far), two, total in zip(items, pairs, weights_of, totals):
+            two = [one.astype(BF16) for one in two]
+            summed = dot(two[0], near[:, wide : 2 * wide]) + dot(two[1], far[:, wide : 2 * wide])
+            result = summed / total
+            rows_out[i, 1, rows, :] = jnp.where(low_part, result[0:count], result[count:size]).astype(BF16)
 
     def spread(i, half):
         rows = slice(half * part, (half + 1) * part)
@@ -579,6 +588,39 @@
         block = rows_in.at[j, 0 : n - 1, pl.ds(half * part, part)]
         remote(block, block, r_send, r_recv.at[j, half], peer).wait_recv()
 
+    def opening(zz, cc):
+        targets = [zt for zt in (CORES * cc, CORES * cc + 1) if zt != zz]
+        targets.sort(key=lambda zt: -abs(zt - zz))
+        for s in range(CUTS):
+            for zt in targets:
+                send_weight(zz, zt, s)
+        for p in range(PIECES):
+            for d in range(2):
+                hop(zz, d, 0, p)
+
+    def reach(zz, d):
+        return zz if d == 0 else n - 1 - zz
+
+    def steps(*names):
+        def script(zz, cc):
+            for kind, k, p in names:
+                if kind == "W":
+                    for far in range(1, n):
+                        for d in range(2):
+                            if far <= reach(zz, d):
+                                event_w(zz - far * way(d), p)
+                elif kind == "Y":
+                    for far in range(1, n):
+                        for d in range(2):
+                            if far <= reach(zz, d):
+                                event_y(zz - far * way(d), p)
+                else:
+                    d = cc if kind == "E" else 1 - cc
+                    if k <= reach(zz, d):
+                        event_x(zz, d, k, p)
+
+        return script
+
     blocks = (
         z,
         z + 1 - 2 * (z % 2),
@@ -586,68 +628,104 @@
         jnp.where(z < 2, 3, 0),
     )
 
-    own = remote(wp.at[z % CORES], wb.at[z], own_send, own_recv, peer)
+    own_w = remote(wp.at[z % CORES], wb.at[z], own_send, own_recv, peer)
     own_local = pltpu.make_async_copy(wp.at[z % CORES], wb.at[z], local_sem.at[12])
     sc = remote(scal.at[c], scal.at[c], sc_send, sc_recv, peer)
-    share = remote(wout.at[:, c], wout.at[:, c], wo_send, wo_recv, peer)
-
-    for p in range(PIECES):
-        send_weights(p)
-        for d in range(2):
-            go(hop(d, 0, p), can_hop(d, 0))
-    go(own, jnp.logical_not(owner) if False else owner)
+
+    def share(j, part):
+        rows = wout.shape[2] // SHARES
+        block = wout.at[j, c, pl.ds(part * rows, rows)]
+        return remote(block, block, wo_send, wo_recv, peer)
+
+    def share_all():
+        pltpu.make_async_copy(wout.at[:, c], wout.at[:, c], local_sem.at[11]).wait()
+        for j in range(2):
+            for part in range(SHARES):
+                share(j, part).start()
+
+
+    run(opening)
+    go(own_w, owner)
     pl.when(owner)(own_local.start)
     go(sc)
-    pltpu.make_async_copy(wout.at[:, c], wout.at[:, c], local_sem.at[11]).wait()
-    go(share)
-
-    for p in range(PIECES):
-        both(event_x, 1, p)
-        for k in range(1, n):
-            both(event_w, k, p)
-        if p:
-            for k in range(1, n):
-                both(event_y, k, p - 1)
-            both(event_x, 2, p - 1)
-    for k in range(1, n):
-        both(event_y, k, PIECES - 1)
-    both(event_x, 2, PIECES - 1)
+
+    run(
+        steps(
+            ("E", 1, 0),
+            ("W", 0, 0),
+            ("E", 1, 1),
+            ("W", 0, 1),
+            ("E", 2, 0),
+            ("E", 1, 2),
+            ("W", 0, 2),
+            ("E", 2, 1),
+            ("E", 1, 3),
+            ("W", 0, 3),
+            ("Y", 0, 0),
+            ("E", 2, 2),
+            ("L", 1, 0),
+            ("E", 2, 3),
+            ("L", 1, 1),
+            ("Y", 0, 1),
+            ("E", 3, 0),
+            ("L", 1, 2),
+            ("E", 3, 1),
+            ("L", 1, 3),
+            ("Y", 0, 2),
+            ("E", 3, 2),
+            ("L", 2, 0),
+            ("E", 3, 3),
+            ("L", 2, 1),
+            ("L", 2, 2),
+            ("L", 2, 3),
+            ("Y", 0, 3),
+        )
+    )
     pl.when(owner)(own_local.wait)
-    pl.when(jnp.logical_not(owner))(own.wait_recv)
+    pl.when(jnp.logical_not(owner))(own_w.wait_recv)
     theirs = wb.at[0 : n - 1, :, 1 - c]
     remote(theirs, theirs, wc_send, wc_recv, peer).wait_recv()
+    run(
+        steps(
+            ("L", 3, 0),
+        )
+    )
     project(blocks[0])
-    go(swap(blocks[0], c))
-    both(event_x, 3, 0)
+    run(
+        steps(
+            ("L", 3, 1),
+        )
+    )
     arrive(blocks[1])
     project(blocks[1])
-    go(swap(blocks[1], c))
-    both(event_x, 3, 1)
-    both(event_x, 3, 2)
-    both(event_x, 3, 3)
+    run(
+        steps(
+            ("L", 3, 2),
+            ("L", 3, 3),
+        )
+    )
     arrive(blocks[2])
     project(blocks[2])
-    go(swap(blocks[2], c))
     remote(scal.at[1 - c], scal.at[1 - c], sc_send, sc_recv, peer).wait_recv()
     for b in blocks[:3]:
         swap(b, 1 - c).wait_recv()
-    early = (jnp.where(z < 2, 1, 3), 2)
-    late = (jnp.where(z < 2, 0, 1), jnp.where(z < 2, 3, 0))
-    for i in early:
-        rows_out[i, 1] = window(i)
+    windows((jnp.where(z < 2, 1, 3), 2), 0, tile)
     arrive(blocks[3])
     project(blocks[3])
-    go(swap(blocks[3], c))
+    share_all()
     swap(blocks[3], 1 - c).wait_recv()
-    for i in late:
-        rows_out[i, 1] = window(i)
     for half in range(HALVES):
         rows = slice(half * part, (half + 1) * part)
-        for i in range(n):
+        windows((jnp.where(z < 2, 0, 1), jnp.where(z < 2, 3, 0)), half * part, part)
+        for i in (3, 0, 2, 1):
             send_rows(i, 1, half)
-        for i in (3, 0, 2, 1):
+        for i in (3, 0):
             rows_out[i, 0, rows, :] = spread(i, half)
-        for i in (3, 0, 2, 1):
+        for i in (3, 0):
+            send_rows(i, 0, half)
+        for i in (2, 1):
+            rows_out[i, 0, rows, :] = spread(i, half)
+        for i in (2, 1):
             send_rows(i, 0, half)
 
     share_in = wout.at[:, 1 - c]

time: 65.6 us -> 62.7 us (0.956)
  Pallas kernels: 64.5 us -> 61.6 us
    pallas_call x1, Pallas kernels: 64.5 us -> 61.6 us  [transposed(): pl.pallas_call(functools.partial(kernel, n), out_shape=pltpu.VMEM((2, til...]
where the time goes in v2:
time: 62.7 us; the launch traced here: 62.5 us
  Pallas kernels  61.6 us (98%)
  local copies, waits for them, and re-layouts  0.97 us (2%)
    pallas_call x1, Pallas kernels, transposed(): pl.pallas_call(functools.partial(kernel, n), out_shape=pltpu.VMEM((2, til...  61.6 us

profile of v2, /device:TPU:0, one launch (start us, length us, event | category | flops | bytes accessed | tf_op | source)
XLA Modules:
  0.0 62.5 jit_solution(5698788177613388140)
XLA Ops:
  0.0 61.6 %shard_map.163 = bf16[2,128,2048]{2,1,0:T(8,128)(2,1)S(1)} custom-call(bf16[2,2,4,16,2048]{4,3,2,1,0:T(8,128)(2,1)} %bitcast.17, bf16[2,2,4,32,256]{4,3,2,1,0:T(8,128)(2,1)} %bitcast.18, bf16[2,2,4,32,256]{4,3,2,1,0:T(8,128)(2,1)} %bitcast.19, bf16[2,2,4,32,256]{4,3,2,1,0:T(8,128)(2,1)} %bitcast.20, bf16[2,2,4,32,256]{4,3,2,1,0:T(8,128)(2,1)} %bitcast.21, ...), custom_call_target="tpu_custom_call" | custom-call | tf_op jit(solution)/shard_map/pallas_call | solution.py:837
  61.6 1.0 %copy.19 = bf16[256,2048]{1,0:T(8,128)(2,1)} copy(bf16[256,2048]{1,0:T(8,128)(2,1)S(1)} %bitcast.16) | data formatting | bytes 2097152

commit v3 on v2

--- a/solution.py
+++ b/solution.py
@@ -206,7 +206,8 @@
 
 PIECES = 4
 CUTS = 4
-HALVES = 2
+EIGHTHS = (0, 3, 8)
+HALVES = len(EIGHTHS) - 1
 COLUMNS = 4
 SHARES = 4
 
@@ -489,7 +490,10 @@
     def mine():
         return scal[z // CORES, z % CORES]
 
-    part = tile // HALVES
+    bounds = [tile * e // 8 for e in EIGHTHS]
+
+    def rows_of(half):
+        return bounds[half], bounds[half + 1] - bounds[half]
 
     def windows(items, start, count):
         rows = slice(start, start + count)
@@ -534,11 +538,12 @@
             rows_out[i, 1, rows, :] = jnp.where(low_part, result[0:count], result[count:size]).astype(BF16)
 
     def spread(i, half):
-        rows = slice(half * part, (half + 1) * part)
+        start, part = rows_of(half)
+        rows = slice(start, start + part)
         size = 2 * part
         q = q_da[i, :, rows, :].reshape(size, wide)
         row = lax.broadcasted_iota(jnp.int32, (size, tile), 0)
-        row = jnp.where(row < part, row, row - part) + half * part
+        row = jnp.where(row < part, row, row - part) + start
         column = lanes((size, tile))
         scores = []
         top = None
@@ -567,7 +572,7 @@
         return rms_norm(blend, head_gain[...]).astype(BF16)
 
     def send_rows(i, j, half):
-        rows = pl.ds(half * part, part)
+        rows = pl.ds(*rows_of(half))
         go(
             remote(
                 rows_out.at[i, j, rows],
@@ -581,11 +586,11 @@
 
         @pl.when(z == i)
         def _():
-            rows = slice(half * part, (half + 1) * part)
+            rows = slice(bounds[half], bounds[half + 1])
             rows_in[j, i, rows, :] = rows_out[i, j, rows, :]
 
     def await_rows(j, half):
-        block = rows_in.at[j, 0 : n - 1, pl.ds(half * part, part)]
+        block = rows_in.at[j, 0 : n - 1, pl.ds(*rows_of(half))]
         remote(block, block, r_send, r_recv.at[j, half], peer).wait_recv()
 
     def opening(zz, cc):
@@ -601,9 +606,9 @@
     def reach(zz, d):
         return zz if d == 0 else n - 1 - zz
 
-    def steps(*names):
+    def steps(ends, mids):
         def script(zz, cc):
-            for kind, k, p in names:
+            for kind, k, p in ends if zz in (0, n - 1) else mids:
                 if kind == "W":
                     for far in range(1, n):
                         for d in range(2):
@@ -649,61 +654,17 @@
     pl.when(owner)(own_local.start)
     go(sc)
 
-    run(
-        steps(
-            ("E", 1, 0),
-            ("W", 0, 0),
-            ("E", 1, 1),
-            ("W", 0, 1),
-            ("E", 2, 0),
-            ("E", 1, 2),
-            ("W", 0, 2),
-            ("E", 2, 1),
-            ("E", 1, 3),
-            ("W", 0, 3),
-            ("Y", 0, 0),
-            ("E", 2, 2),
-            ("L", 1, 0),
-            ("E", 2, 3),
-            ("L", 1, 1),
-            ("Y", 0, 1),
-            ("E", 3, 0),
-            ("L", 1, 2),
-            ("E", 3, 1),
-            ("L", 1, 3),
-            ("Y", 0, 2),
-            ("E", 3, 2),
-            ("L", 2, 0),
-            ("E", 3, 3),
-            ("L", 2, 1),
-            ("L", 2, 2),
-            ("L", 2, 3),
-            ("Y", 0, 3),
-        )
-    )
+    run(steps((("E", 1, 0), ("W", 0, 0), ("E", 1, 1), ("W", 0, 1), ("E", 1, 2), ("E", 2, 0), ("E", 1, 3), ("E", 2, 1), ("W", 0, 2), ("L", 1, 0), ("E", 2, 2), ("L", 1, 1), ("W", 0, 3), ("L", 1, 2), ("Y", 0, 0), ("E", 2, 3), ("L", 1, 3), ("Y", 0, 1), ("E", 3, 0), ("E", 3, 1), ("Y", 0, 2), ("E", 3, 2), ("L", 2, 0), ("E", 3, 3), ("L", 2, 1), ("L", 2, 2), ("L", 2, 3), ("Y", 0, 3)), (("E", 1, 0), ("W", 0, 0), ("E", 1, 1), ("W", 0, 1), ("E", 1, 2), ("E", 1, 3), ("W", 0, 2), ("E", 2, 0), ("E", 2, 1), ("W", 0, 3), ("L", 1, 0), ("E", 2, 2), ("L", 1, 1), ("E", 2, 3), ("L", 1, 2), ("Y", 0, 0), ("L", 1, 3), ("Y", 0, 1), ("L", 2, 0), ("Y", 0, 2), ("L", 2, 1), ("L", 2, 2), ("L", 2, 3), ("Y", 0, 3))))
     pl.when(owner)(own_local.wait)
     pl.when(jnp.logical_not(owner))(own_w.wait_recv)
     theirs = wb.at[0 : n - 1, :, 1 - c]
     remote(theirs, theirs, wc_send, wc_recv, peer).wait_recv()
-    run(
-        steps(
-            ("L", 3, 0),
-        )
-    )
+    run(steps((("L", 3, 0),), ()))
     project(blocks[0])
-    run(
-        steps(
-            ("L", 3, 1),
-        )
-    )
+    run(steps((("L", 3, 1),), ()))
     arrive(blocks[1])
     project(blocks[1])
-    run(
-        steps(
-            ("L", 3, 2),
-            ("L", 3, 3),
-        )
-    )
+    run(steps((("L", 3, 2), ("L", 3, 3)), ()))
     arrive(blocks[2])
     project(blocks[2])
     remote(scal.at[1 - c], scal.at[1 - c], sc_send, sc_recv, peer).wait_recv()
@@ -715,8 +676,8 @@
     share_all()
     swap(blocks[3], 1 - c).wait_recv()
     for half in range(HALVES):
-        rows = slice(half * part, (half + 1) * part)
-        windows((jnp.where(z < 2, 0, 1), jnp.where(z < 2, 3, 0)), half * part, part)
+        rows = slice(bounds[half], bounds[half + 1])
+        windows((jnp.where(z < 2, 0, 1), jnp.where(z < 2, 3, 0)), *rows_of(half))
         for i in (3, 0, 2, 1):
             send_rows(i, 1, half)
         for i in (3, 0):
@@ -733,7 +694,7 @@
     columns = out_ref.shape[2] // COLUMNS
 
     def span(half, q):
-        return pl.ds(half * part, part), pl.ds(q * columns, columns)
+        return pl.ds(*rows_of(half)), pl.ds(q * columns, columns)
 
     def summing(half, q):
         rows, cols = span(half, q)
@@ -753,7 +714,7 @@
         go(remote(block, block, o_send, o_recv, peer))
 
     for half in range(HALVES):
-        rows = slice(half * part, (half + 1) * part)
+        rows = slice(bounds[half], bounds[half + 1])
         await_rows(1, half)
         await_rows(0, half)
         for q in range(COLUMNS):

time: 62.7 us -> 61.6 us (0.982)
  Pallas kernels: 61.6 us -> 60.5 us
    pallas_call x1, Pallas kernels: 61.6 us -> 60.5 us  [transposed(): pl.pallas_call(functools.partial(kernel, n), out_shape=pltpu.VMEM((2, til...]
where the time goes in v3:
time: 61.6 us; the launch traced here: 61.4 us
  Pallas kernels  60.5 us (98%)
  local copies, waits for them, and re-layouts  0.97 us (2%)
    pallas_call x1, Pallas kernels, transposed(): pl.pallas_call(functools.partial(kernel, n), out_shape=pltpu.VMEM((2, til...  60.5 us

profile of v3, /device:TPU:0, one launch (start us, length us, event | category | flops | bytes accessed | tf_op | source)
XLA Modules:
  0.0 61.4 jit_solution(9495664733318739926)
XLA Ops:
  0.0 60.5 %shard_map.163 = bf16[2,128,2048]{2,1,0:T(8,128)(2,1)S(1)} custom-call(bf16[2,2,4,16,2048]{4,3,2,1,0:T(8,128)(2,1)} %bitcast.17, bf16[2,2,4,32,256]{4,3,2,1,0:T(8,128)(2,1)} %bitcast.18, bf16[2,2,4,32,256]{4,3,2,1,0:T(8,128)(2,1)} %bitcast.19, bf16[2,2,4,32,256]{4,3,2,1,0:T(8,128)(2,1)} %bitcast.20, bf16[2,2,4,32,256]{4,3,2,1,0:T(8,128)(2,1)} %bitcast.21, ...), custom_call_target="tpu_custom_call" | custom-call | tf_op jit(solution)/shard_map/pallas_call | solution.py:798
  60.5 1.0 %copy.19 = bf16[256,2048]{1,0:T(8,128)(2,1)} copy(bf16[256,2048]{1,0:T(8,128)(2,1)S(1)} %bitcast.16) | data formatting | bytes 2097152

commit v4 on v3

--- a/solution.py
+++ b/solution.py
@@ -386,11 +386,11 @@
         source, target = zz - k * way(d), zz + way(d)
         if 0 <= target < n:
             piece = xg.at[source, x, p]
-            remote(piece, piece, x_send.at[d], x_recv.at[d, k, p], {"sp": target}).start()
+            remote(piece, piece, x_send.at[d], x_recv.at[(source - target - 1) % n, p], {"sp": target}).start()
 
     def weight_beside(zs, yy, s):
         piece = wb.at[zs, yy, c, s]
-        return remote(piece, piece, wy_send, wy_recv.at[zs, s], beside)
+        return remote(piece, piece, wy_send, wy_recv.at[(zs - z - 1 + n) % n, s], beside)
 
     def weight_core(zs, yy, s):
         piece = wb.at[zs, yy, c, s]
@@ -399,14 +399,14 @@
     def event_x(zz, d, k, p):
         zs = zz - k * way(d)
         piece = xg.at[zs, x, p]
-        remote(piece, piece, x_send.at[d], x_recv.at[d, k - 1, p], across).wait_recv()
+        remote(piece, piece, x_send.at[d], x_recv.at[(zs - zz - 1) % n, p], across).wait_recv()
         if k < n - 1:
             hop(zz, d, k, p)
         cross(zs, p).start()
 
     def event_w(zs, s):
         piece = wb.at[zs, y, c, s]
-        remote(piece, piece, w_send, w_recv.at[zs, s], peer).wait_recv()
+        remote(piece, piece, w_send, w_recv.at[(zs - z - 1 + n) % n, s], peer).wait_recv()
         weight_beside(zs, y, s).start()
         weight_core(zs, y, s).start()
 
@@ -420,7 +420,7 @@
                 wp.at[zt % CORES, y, cd, s],
                 wb.at[zz, y, cd, s],
                 w_send,
-                w_recv.at[zz, s],
+                w_recv.at[(zz - zt - 1) % n, s],
                 at(zt, cd),
             ).start()
 
@@ -823,15 +823,15 @@
             pltpu.VMEM((2, n, tile, wide), BF16),
             pltpu.VMEM((tile, d), BF16),
             pltpu.VMEM((tile, d), BF16),
-            DMA((14,)),
+            DMA((13,)),
             DMA((2,)),
-            DMA((2, n - 1, PIECES)),
+            DMA((n - 1, PIECES)),
             DMA,
             DMA((n,)),
             DMA,
-            DMA((n, CUTS)),
-            DMA,
-            DMA((n, CUTS)),
+            DMA((n - 1, CUTS)),
+            DMA,
+            DMA((n - 1, CUTS)),
             DMA,
             DMA,
             DMA,

time: 61.6 us -> 61.4 us (level)
  no operation moved by 1% of the time
where the time goes in v4:
time: 61.4 us; the launch traced here: 61.3 us
  Pallas kernels  60.3 us (98%)
  local copies, waits for them, and re-layouts  0.97 us (2%)
    pallas_call x1, Pallas kernels, transposed(): pl.pallas_call(functools.partial(kernel, n), out_shape=pltpu.VMEM((2, til...  60.3 us

profile of v4, /device:TPU:0, one launch (start us, length us, event | category | flops | bytes accessed | tf_op | source)
XLA Modules:
  0.0 61.3 jit_solution(18347020914160477520)
XLA Ops:
  0.0 60.3 %shard_map.163 = bf16[2,128,2048]{2,1,0:T(8,128)(2,1)S(1)} custom-call(bf16[2,2,4,16,2048]{4,3,2,1,0:T(8,128)(2,1)} %bitcast.17, bf16[2,2,4,32,256]{4,3,2,1,0:T(8,128)(2,1)} %bitcast.18, bf16[2,2,4,32,256]{4,3,2,1,0:T(8,128)(2,1)} %bitcast.19, bf16[2,2,4,32,256]{4,3,2,1,0:T(8,128)(2,1)} %bitcast.20, bf16[2,2,4,32,256]{4,3,2,1,0:T(8,128)(2,1)} %bitcast.21, ...), custom_call_target="tpu_custom_call" | custom-call | tf_op jit(solution)/shard_map/pallas_call | solution.py:798
  60.3 1.0 %copy.19 = bf16[256,2048]{1,0:T(8,128)(2,1)} copy(bf16[256,2048]{1,0:T(8,128)(2,1)S(1)} %bitcast.16) | data formatting | bytes 2097152
